TPU v7x, 32 devices: a whole 2x2x4 slice. The times are simulated.
32 devices in a mesh: fs: 16 (over z, y, x), tp: 2 (over core).
Axes of the slice: x: 2, y: 2, z: 4, core: 2. Of those that a mesh axis runs over, the one named last changes fastest.
Arguments:
- tokens: bfloat16 [4096, 1024], P('fs', 'tp'), may hold values from -6 to 6
- mix_gain: float32 [1024], replicated, may hold values from 0.1 to 1.9
- mix_value_w: float32 [1024, 1024], P('fs', 'tp'), may hold values from -0.1875 to 0.1875
- mix_gate_w: float32 [1024, 1024], P('fs', 'tp'), may hold values from -0.1875 to 0.1875
- mix_kernel: float32 [31, 1024], P(None, 'tp'), may hold values from -1 to 1
- chan_gain: float32 [1024], P('tp'), may hold values from 0.1 to 1.9
- chan_bias: float32 [1024], P('tp'), may hold values from -3 to 3
- mix_out_w: float32 [1024, 1024], P('tp', 'fs'), may hold values from -0.1875 to 0.1875
- ffn_gain: float32 [1024], replicated, may hold values from 0.1 to 1.9
- ffn_value_w: float32 [1024, 2560], P('fs', 'tp'), may hold values from -0.1875 to 0.1875
- ffn_gate_w: float32 [1024, 2560], P('fs', 'tp'), may hold values from -0.1875 to 0.1875
- ffn_value_kernel: float32 [3, 2560], P(None, 'tp'), may hold values from -3.5 to 3.5
- ffn_gate_kernel: float32 [3, 2560], P(None, 'tp'), may hold values from -3.5 to 3.5
- ffn_down_w: float32 [2560, 1024], P('tp', 'fs'), may hold values from -0.125 to 0.125
Outputs:
- layer_out: bfloat16 [4096, 1024], P('fs', 'tp')
All inputs are finite; a program needn't handle non-finite values.
Results may differ from a plain program's by a relative error of at most 0.0035.
Values may be sent and summed in bfloat16 or wider, within the bound.
A program may use at most 64 MiB of HBM per device.

v0:
```python
import jax
import jax.numpy as jnp
from jax import lax
from jax.sharding import PartitionSpec as P

CONV_W = 1024
SEQ_LEN = 32


EPS = 1e-06


def rms_rows(act_rows, norm_gain):
    values = act_rows.astype(jnp.float32)
    scaled = values * lax.rsqrt(jnp.mean(values * values, axis=-1, keepdims=True) + EPS)
    return (scaled * norm_gain).astype(jnp.bfloat16)


def along_positions(values, kernel, length):
    seq_count = values.shape[0] // length
    blocks = values.reshape(seq_count, length, values.shape[1])
    half_width = kernel.shape[0] // 2
    padded = jnp.pad(blocks, ((0, 0), (half_width, half_width), (0, 0)))
    summed = jnp.zeros_like(blocks)
    for offset in range(kernel.shape[0]):
        summed = summed + padded[:, offset : offset + length, :] * kernel[offset]
    return summed.reshape(values.shape)


def collect_rows(local_rows):
    return lax.all_gather(local_rows, "tp", axis=1, tiled=True)


def project_in(normed, weight_one, weight_two):
    empty = jnp.zeros((normed.shape[0], weight_one.shape[1]), jnp.float32)

    def add_both(totals, pieces):
        columns = lax.slice_in_dim(normed, 0, pieces[0].shape[0], axis=1)
        first = totals[0] + jnp.dot(
            columns, pieces[0].astype(jnp.bfloat16), preferred_element_type=jnp.float32
        )
        second = totals[1] + jnp.dot(
            columns, pieces[1].astype(jnp.bfloat16), preferred_element_type=jnp.float32
        )
        return (first, second)

    return add_both(
        (empty, empty),
        (
            lax.all_gather(weight_one.astype(jnp.bfloat16), "fs", axis=0, tiled=True),
            lax.all_gather(weight_two.astype(jnp.bfloat16), "fs", axis=0, tiled=True),
        ),
    )


def project_out(active, weight):

    def apply_piece(piece):
        return jnp.dot(active, piece.astype(jnp.bfloat16), preferred_element_type=jnp.float32)

    partial_terms = apply_piece(lax.all_gather(weight.astype(jnp.bfloat16), "fs", axis=1, tiled=True))
    return lax.psum_scatter(partial_terms, "tp", scatter_dimension=1, tiled=True)


def body(
    tokens,
    mix_gain,
    mix_value_w,
    mix_gate_w,
    mix_kernel,
    chan_gain,
    chan_bias,
    mix_out_w,
    ffn_gain,
    ffn_value_w,
    ffn_gate_w,
    ffn_value_kernel,
    ffn_gate_kernel,
    ffn_down_w,
):
    normed = rms_rows(collect_rows(tokens), mix_gain)
    mix_value, mix_gate = project_in(normed, mix_value_w, mix_gate_w)
    glu_rows = mix_value * jax.nn.sigmoid(mix_gate)
    mixed = along_positions(glu_rows, mix_kernel, SEQ_LEN)
    chan_sum, chan_square = lax.psum(
        (jnp.sum(mixed, axis=-1), jnp.sum(mixed * mixed, axis=-1)), "tp"
    )
    chan_mean = (chan_sum / CONV_W)[:, None]
    chan_var = jnp.maximum((chan_square / CONV_W)[:, None] - chan_mean * chan_mean, 0.0)
    active = jax.nn.silu(
        (mixed - chan_mean) * lax.rsqrt(chan_var + EPS) * chan_gain + chan_bias
    ).astype(jnp.bfloat16)
    middle = (tokens.astype(jnp.float32) + project_out(active, mix_out_w)).astype(jnp.bfloat16)
    normed_ffn = rms_rows(collect_rows(middle), ffn_gain)
    up_value, up_gate = project_in(normed_ffn, ffn_value_w, ffn_gate_w)
    up_value = along_positions(up_value, ffn_value_kernel, SEQ_LEN)
    up_gate = along_positions(up_gate, ffn_gate_kernel, SEQ_LEN)
    hidden = (jax.nn.silu(up_gate) * up_value).astype(jnp.bfloat16)
    return (middle.astype(jnp.float32) + project_out(hidden, ffn_down_w)).astype(jnp.bfloat16)


def solution(mesh):
    return jax.shard_map(
        body,
        mesh=mesh,
        in_specs=(
            P("fs", "tp"),
            P(),
            P("fs", "tp"),
            P("fs", "tp"),
            P(None, "tp"),
            P("tp"),
            P("tp"),
            P("tp", "fs"),
            P(),
            P("fs", "tp"),
            P("fs", "tp"),
            P(None, "tp"),
            P(None, "tp"),
            P("tp", "fs"),
        ),
        out_specs=P("fs", "tp"),
        check_vma=False,
    )
```

profile of v0, /device:TPU:0, one launch (start us, length us, event | category | flops | bytes accessed | tf_op | source)
XLA Modules:
  0.0 410.3 jit_solution(10366963727027574228)
XLA Ops:
  6.5 1.6 convert_element_type.57
  8.2 1.5 convert_element_type.56
  9.8 1.5 convert_element_type.59
  11.4 2.5 all_gather.24
  14.2 53.7 %all-gather.9.cloned.1.call-done = bf16[1024,512]{1,0:T(8,128)(2,1)} async-done(((bf16[64,512]{1,0:T(8,128)(2,1)}), bf16[1024,512]{1,0:T(8,128)(2,1)}) %all-gather.9.cloned.1.call-update) | async-done | bytes 1048592 | tf_op jit(solution)/shard_map/all_gather | solution.py:51
  67.9 1.8 fusion.14
  69.8 54.9 %all-gather.7.cloned.1.call-done = bf16[1024,512]{1,0:T(8,128)(2,1)} async-done(((bf16[64,512]{1,0:T(8,128)(2,1)}), bf16[1024,512]{1,0:T(8,128)(2,1)}) %all-gather.7.cloned.1.call-update) | async-done | bytes 1048592 | tf_op jit(solution)/shard_map/all_gather | solution.py:50
  124.7 1.7 convolution_multiply_fusion
  126.4 2.4 fusion.90
  128.9 2.4 all-reduce.3
  131.7 49.7 %all-gather.11.cloned.1.call-done = bf16[512,1024]{0,1:T(8,128)(2,1)} async-done(((bf16[512,64]{0,1:T(8,128)(2,1)}), bf16[512,1024]{0,1:T(8,128)(2,1)}) %all-gather.11.cloned.1.call-update) | async-done | bytes 1048592 | tf_op jit(solution)/shard_map/all_gather | solution.py:61
  181.4 2.8 fusion.94
  186.8 4.8 %reduce-scatter.3.cloned.1.call-done = f32[256,512]{1,0:T(8,128)} async-done(((f32[256,1024]{1,0:T(8,128)}), f32[256,512]{1,0:T(8,128)}) %reduce-scatter.3.cloned.1.call-update) | async-done | bytes 524304 | tf_op jit(solution)/shard_map/reduce_scatter | solution.py:62
  191.6 1.1 add_convert_fusion.1
  192.7 2.2 all_gather.28
  195.1 64.4 %all-gather.15.cloned.1.call-done = bf16[1024,1280]{1,0:T(8,128)(2,1)} async-done(((bf16[64,1280]{1,0:T(8,128)(2,1)}), bf16[1024,1280]{1,0:T(8,128)(2,1)}) %all-gather.15.cloned.1.call-update) | async-done | bytes 2621456 | tf_op jit(solution)/shard_map/all_gather | solution.py:50
  259.5 2.6 fusion.84
  262.2 62.9 %all-gather.13.cloned.1.call-done = bf16[1024,1280]{1,0:T(8,128)(2,1)} async-done(((bf16[64,1280]{1,0:T(8,128)(2,1)}), bf16[1024,1280]{1,0:T(8,128)(2,1)}) %all-gather.13.cloned.1.call-update) | async-done | bytes 2621456 | tf_op jit(solution)/shard_map/all_gather | solution.py:51
  325.0 2.6 fusion.86
  327.7 0.8 fusion.2
  328.8 61.8 %all-gather.17.cloned.1.call-done = bf16[1280,1024]{0,1:T(8,128)(2,1)} async-done(((bf16[1280,64]{0,1:T(8,128)(2,1)}), bf16[1280,1024]{0,1:T(8,128)(2,1)}) %all-gather.17.cloned.1.call-update) | async-done | bytes 2621456 | tf_op jit(solution)/shard_map/all_gather | solution.py:61
  390.7 3.6 fusion.95
  394.3 7.3 %reduce-scatter.5.cloned.1.call-done = f32[256,512]{1,0:T(8,128)} async-done(((f32[256,1024]{1,0:T(8,128)}), f32[256,512]{1,0:T(8,128)}) %reduce-scatter.5.cloned.1.call-update) | async-done | bytes 524304 | tf_op jit(solution)/shard_map/reduce_scatter | solution.py:62
  401.6 1.8 add_convert_fusion
  (54 shorter events, 4.0 us)
Async XLA Ops:
  6.5 7.6 %copy-start.5 = (f32[31,512]{1,0:T(8,128)S(1)}, f32[31,512]{1,0:T(8,128)}, u32[]{:S(2)}) copy-start(f32[31,512]{1,0:T(8,128)} %param.18) | copy-start | bytes 190468
  6.5 61.4 %copy-start.8 = (f32[1024]{0:T(1024)S(1)}, f32[1024]{0:T(1024)}, u32[]{:S(2)}) copy-start(f32[1024]{0:T(1024)} %param.15) | copy-start | bytes 12292
  6.5 61.4 %all-gather.9.cloned.1.call-start = ((), (), s32[]{:S(2)}) async-start(), calls=%async_computation.3 | async-start | bytes 1114112 | tf_op jit(solution)/shard_map/all_gather | solution.py:51
  8.1 116.5 %all-gather.7.cloned.1.call-start = ((), (), s32[]{:S(2)}) async-start(), calls=%async_computation.2 | async-start | bytes 1114112 | tf_op jit(solution)/shard_map/all_gather | solution.py:50
  9.8 171.6 %all-gather.11.cloned.1.call-start = ((), (), s32[]{:S(2)}) async-start(), calls=%async_computation.4 | async-start | bytes 1114112 | tf_op jit(solution)/shard_map/all_gather | solution.py:61
  11.4 180.2 %reduce-scatter.3.cloned.1.call-start = ((), (), s32[]{:S(2)}) async-start(), calls=%async_computation.5 | async-start | bytes 1572864 | tf_op jit(solution)/shard_map/reduce_scatter | solution.py:62
  69.7 61.7 %copy-start.9 = (f32[512]{0:T(512)S(1)}, f32[512]{0:T(512)}, u32[]{:S(2)}) copy-start(f32[512]{0:T(512)} %param.20) | copy-start | bytes 6148
  69.7 61.6 %copy-start.10 = (f32[512]{0:T(512)S(1)}, f32[512]{0:T(512)}, u32[]{:S(2)}) copy-start(f32[512]{0:T(512)} %param.19) | copy-start | bytes 6148
  131.7 52.6 %copy-start.1 = (f32[64,1280]{1,0:T(8,128)S(1)}, f32[64,1280]{1,0:T(8,128)}, u32[]{:S(2)}) copy-start(f32[64,1280]{1,0:T(8,128)} %param.23) | copy-start | bytes 983044
  184.2 1.0 copy-start.2
  184.2 1.7 copy-start.3
  184.2 2.5 copy-start.6
  184.2 2.6 copy-start.7
  184.2 7.4 %copy-start = (bf16[256,512]{1,0:T(8,128)(2,1)S(1)}, bf16[256,512]{1,0:T(8,128)(2,1)}, u32[]{:S(2)}) copy-start(bf16[256,512]{1,0:T(8,128)(2,1)} %param.14) | copy-start | bytes 786436
  184.2 75.3 %all-gather.15.cloned.1.call-start = ((), (), s32[]{:S(2)}) async-start(), calls=%async_computation.7 | async-start | bytes 2785280 | tf_op jit(solution)/shard_map/all_gather | solution.py:50
  185.0 140.0 %all-gather.13.cloned.1.call-start = ((), (), s32[]{:S(2)}) async-start(), calls=%async_computation.6 | async-start | bytes 2785280 | tf_op jit(solution)/shard_map/all_gather | solution.py:51
  185.8 204.8 %all-gather.17.cloned.1.call-start = ((), (), s32[]{:S(2)}) async-start(), calls=%async_computation.8 | async-start | bytes 2785280 | tf_op jit(solution)/shard_map/all_gather | solution.py:61
  186.6 72.9 %copy-start.4 = (f32[1024]{0:T(1024)S(1)}, f32[1024]{0:T(1024)}, u32[]{:S(2)}) copy-start(f32[1024]{0:T(1024)} %param.22) | copy-start | bytes 12292
  186.6 215.0 %reduce-scatter.5.cloned.1.call-start = ((), (), s32[]{:S(2)}) async-start(), calls=%async_computation.9 | async-start | bytes 1572864 | tf_op jit(solution)/shard_map/reduce_scatter | solution.py:62
Sparse Core Ops, SparseCore 0:
  10.1 57.8 all-gather.8
  70.7 53.9 all-gather.6
  127.4 53.9 all-gather.10
  184.3 7.2 reduce-scatter.2
  194.2 65.3 all-gather.14
  262.1 62.9 all-gather.12
  327.7 62.9 all-gather.16
  394.4 7.1 reduce-scatter.4
where the time goes:
time: 411 us; the launch traced here: 410 us
  waiting for transfers between devices  360 us (88%)
  matrix products  15.1 us (4%)
  other arithmetic  13.9 us (3%)
  between operations  13.7 us (3%)
  blocking collectives  7.17 us (2%)
    all_gather x2, waiting for transfers between devices, project_in(): lax.all_gather(weight_one.astype(jnp.bfloat16), 'fs', axis=0, tiled=True)  119 us
    all_gather x2, waiting for transfers between devices, project_in(): lax.all_gather(weight_two.astype(jnp.bfloat16), 'fs', axis=0, tiled=True)  117 us
    all_gather x2, waiting for transfers between devices, project_out(): lax.all_gather(weight.astype(jnp.bfloat16), 'fs', axis=1, tiled=True)  112 us
    reduce_scatter x2, waiting for transfers between devices, project_out(): lax.psum_scatter(partial_terms, 'tp', scatter_dimension=1, tiled=True)  12.1 us
  transfers between devices with their start and end apart: 8, of which 8 were waited for; matrix products, arithmetic and copies ran while one was open for 5% of the time, Pallas kernels for 0%

commit v1 on v0

--- a/solution.py
+++ b/solution.py
@@ -1,6 +1,10 @@
+import functools
+
 import jax
 import jax.numpy as jnp
 from jax import lax
+from jax.experimental import pallas as pl
+from jax.experimental.pallas import tpu as pltpu
 from jax.sharding import PartitionSpec as P
 
 CONV_W = 1024
@@ -99,9 +103,508 @@
     return (middle.astype(jnp.float32) + project_out(hidden, ffn_down_w)).astype(jnp.bfloat16)
 
 
+MESH = pl.DeviceIdType.MESH
+UNIT_US = 0.36
+HOP_US = 1.8
+
+
+def chunk_plan(mix_cols, ffn_cols):
+    unit = 256
+    first = max(unit, (2 * ffn_cols // 5) // unit * unit)
+    rest = ffn_cols - 2 * first
+    plan = [
+        ("mv", "A", mix_cols, True),
+        ("mg", "B", mix_cols, True),
+        ("v0", "A", first, False),
+        ("g0", "B", first, False),
+        ("mo", "D", mix_cols, False),
+        ("v1", "A", first, False),
+        ("g1", "B", first, False),
+        ("w0", "A", first, False),
+        ("w1", "B", first, False),
+        ("vg2", "E", 2 * rest, False),
+        ("w2", "D", rest, False),
+    ]
+    gates = {
+        "v1": ("mo", "u", 2),
+        "g1": ("mo", "u", 2),
+        "w0": ("v1", "u", 1),
+        "w1": ("g1", "u", 1),
+        "vg2": ("w0", "u", 2),
+        "w2": ("vg2", "u", 1),
+    }
+    return plan, gates
+
+
+def build_transfers(plan, gates, line):
+    out = {}
+    for name, kind, cols, fine in plan:
+        width = cols // 128
+        gate = [gates[name]] if name in gates else []
+        steps = range(1, line)
+        if kind in "AB":
+            one, two = ("y", "x") if kind == "A" else ("x", "y")
+            for t in steps:
+                for d in "ud":
+                    deps = [(name, d, t - 1)] if t > 1 else gate
+                    out[(name, d, t)] = dict(link="z" + d, size=width, deps=deps, phase="z")
+            everything = [(name, d, t) for t in steps for d in "ud"]
+            if fine:
+                out[(name, "1", "o", 0)] = dict(link=one, size=width, deps=[], phase="f1", axis=one)
+                out[(name, "2", "o", 0)] = dict(
+                    link=two, size=2 * width, deps=[(name, "1", "o", 0)], phase="f2", axis=two
+                )
+                for _, d, t in everything:
+                    out[(name, "1", d, t)] = dict(link=one, size=width, deps=[(name, d, t)], phase="f1", axis=one)
+                    out[(name, "2", d, t)] = dict(
+                        link=two, size=2 * width, deps=[(name, "1", d, t)], phase="f2", axis=two
+                    )
+            else:
+                out[(name, "1")] = dict(link=one, size=line * width, deps=everything, phase="c1", axis=one)
+                out[(name, "2")] = dict(link=two, size=2 * line * width, deps=[(name, "1")], phase="c2", axis=two)
+        else:
+            one, two = ("x", "y") if kind == "D" else ("y", "x")
+            out[(name, "1")] = dict(link=one, size=width, deps=[], phase="p1", axis=one)
+            out[(name, "2")] = dict(link=two, size=2 * width, deps=[(name, "1")], phase="p2", axis=two)
+            for t in steps:
+                for d in "ud":
+                    deps = [(name, d, t - 1)] if t > 1 else [(name, "2")] + gate
+                    out[(name, d, t)] = dict(link="z" + d, size=4 * width, deps=deps, phase="q")
+    return out
+
+
+def order_events(transfers, computes):
+    free, arrival, seen, done = {}, {}, set(), set()
+    program, now = [], 0.0
+
+    def issue():
+        for key, item in transfers.items():
+            if key not in arrival and all(dep in seen for dep in item["deps"]):
+                start = max(now, free.get(item["link"], 0.0))
+                free[item["link"]] = start + item["size"] * UNIT_US
+                arrival[key] = free[item["link"]] + HOP_US
+                program.append(("send", key))
+
+    issue()
+    program.append(("local", None))
+    while len(seen) < len(transfers) or len(done) < len(computes):
+        waiting = sorted((arrival[key], i, key) for i, key in enumerate(transfers) if key in arrival and key not in seen)
+        ready = None
+        for name, needs, after, cost in computes:
+            if name in done:
+                continue
+            chunk_ok = all(key in seen for key in transfers if key[0] in needs)
+            if chunk_ok and all(a in done for a in after):
+                ready = (name, cost)
+                break
+        if waiting and waiting[0][0] <= now or (waiting and ready is None):
+            now = max(now, waiting[0][0])
+            seen.add(waiting[0][2])
+            program.append(("recv", waiting[0][2]))
+            issue()
+        else:
+            program.append(("compute", ready[0]))
+            now += ready[1]
+            done.add(ready[0])
+    return program
+
+
+def compute_list(groups):
+    items = [
+        ("norm1", (), (), 1.0),
+        ("mixv", ("mv",), ("norm1",), 0.8),
+        ("mixg", ("mg",), ("mixv",), 1.0),
+        ("conv_a", (), ("mixg",), 1.5),
+        ("conv_b", (), ("conv_a",), 1.5),
+        ("stats", (), ("conv_b",), 0.5),
+        ("active", (), ("stats",), 1.5),
+        ("out_peer", ("mo",), ("active",), 0.6),
+        ("out_mine", (), ("out_peer",), 0.6),
+        ("middle", (), ("out_mine",), 1.0),
+        ("norm2", (), ("middle",), 1.5),
+        ("up0", ("v0", "g0"), ("norm2",), 2.0),
+        ("up1", ("v1", "g1"), ("norm2",), 2.0),
+        ("up2", ("vg2",), ("norm2",), 1.0),
+    ]
+    for g in (0, 1, 2):
+        items.append(("down_peer%d" % g, ("w%d" % g,), ("up%d" % g,), 0.5))
+    items.append(("send_down", (), tuple("down_peer%d" % g for g in (0, 1, 2)), 0.1))
+    for g in (0, 1, 2):
+        items.append(("down_mine%d" % g, (), ("send_down",), 0.5))
+    items.append(("finish", (), tuple("down_mine%d" % g for g in (0, 1, 2)), 1.0))
+    return items
+
+
+def layer_kernel(sizes, plan, transfers, program, *refs):
+    line, rows, tok_rows, mix_cols, ffn_cols, width, taps, ffn_taps = sizes
+    (tokens, gain1, kern, cgain, cbias, gain2, vkern, gkern, packed) = refs[:9]
+    out = refs[9]
+    scratch = refs[10:]
+    held = {item[0]: scratch[i] for i, item in enumerate(plan)}
+    (tok_peer, normed, mvbuf, pad, mixed, stat, stat_peer, active, part_send, part_mine, part_recv,
+     middle, mid_peer, hid0, hid1, hid2, down_send, down_mine, down_recv,
+     send_sem, recv_sem, loc_sem, tp_send, tp_recv) = scratch[len(plan):]
+    hidden = (hid0, hid1, hid2)
+    offsets, at = {}, 0
+    for name, _, cols, _ in plan:
+        offsets[name] = at
+        at += cols
+    cols_of = {item[0]: item[2] for item in plan}
+    numbers = {key: i for i, key in enumerate(transfers)}
+    fs = lax.axis_index("fs")
+    core = lax.axis_index("tp")
+    peer = 1 - core
+    z, y, x = lax.div(fs, 4), lax.rem(lax.div(fs, 2), 2), lax.rem(fs, 2)
+    at_y, at_x = fs + 2 - 4 * y, fs + 1 - 2 * x
+    half = line // 2
+
+    barrier = pltpu.get_barrier_semaphore()
+    for dev in ({"fs": at_y}, {"fs": at_x}, {"tp": peer}):
+        pl.semaphore_signal(barrier, inc=1, device_id=dev, device_id_type=MESH)
+
+    @pl.when(z > 0)
+    def _():
+        pl.semaphore_signal(barrier, inc=1, device_id={"fs": fs - 4}, device_id_type=MESH)
+
+    @pl.when(z < line - 1)
+    def _():
+        pl.semaphore_signal(barrier, inc=1, device_id={"fs": fs + 4}, device_id_type=MESH)
+
+    local = []
+    for i, (name, _, cols, _) in enumerate(plan):
+        copy = pltpu.make_async_copy(
+            packed.at[:, pl.ds(offsets[name], cols)], held[name].at[z, y, x], loc_sem.at[i]
+        )
+        copy.start()
+        local.append(copy)
+    pl.semaphore_wait(barrier, 3 + jnp.minimum(z, 1) + jnp.minimum(line - 1 - z, 1))
+
+    def guards(key, sending):
+        phase = transfers[key]["phase"]
+        if phase in ("z", "q"):
+            d, t = key[1], key[2]
+            if d == "u":
+                return jnp.logical_and(z >= t - 1, z < line - 1) if sending else z >= t
+            return jnp.logical_and(z <= line - t, z > 0) if sending else z <= line - 1 - t
+        if phase in ("f1", "f2") and key[2] != "o":
+            d, t = key[2], key[3]
+            return z >= t if d == "u" else z <= line - 1 - t
+        return None
+
+    def make(key, sending):
+        item = transfers[key]
+        phase, name, i = item["phase"], key[0], numbers[key]
+        buf = held[name]
+        own = packed.at[:, pl.ds(offsets[name], cols_of[name])]
+        src = None
+        if phase in ("z", "q"):
+            d, t = key[1], key[2]
+            back = t - 1 if sending else t
+            block = z - back if d == "u" else z + back
+            dev = {"fs": fs + 4 if d == "u" else fs - 4}
+            if phase == "z":
+                dst = buf.at[block, y, x]
+                src = own if sending and t == 1 else dst
+            else:
+                dst = buf.at[block]
+        else:
+            axis = item["axis"]
+            dev = {"fs": at_y if axis == "y" else at_x}
+            yy, xx = y, x
+            if not sending:
+                yy, xx = (1 - y, x) if axis == "y" else (y, 1 - x)
+            if phase in ("f1", "f2"):
+                d, t = key[2], key[3]
+                block = z - t if d == "u" else z + t
+            elif phase in ("p1", "p2"):
+                block = z
+            else:
+                block = slice(None)
+            if phase in ("f1", "p1", "c1"):
+                dst = buf.at[block, yy, xx]
+                if sending and (phase == "p1" or (phase == "f1" and key[2] == "o")):
+                    src = own
+            elif axis == "x":
+                dst = buf.at[block, :, xx]
+            else:
+                dst = buf.at[block, yy, :]
+        return pltpu.make_async_remote_copy(
+            src_ref=dst if src is None else src, dst_ref=dst, send_sem=send_sem.at[i],
+            recv_sem=recv_sem.at[i], device_id=dev, device_id_type=MESH,
+        )
+
+    def act(key, sending, what):
+        guard = guards(key, sending)
+
+        def run():
+            what(make(key, sending))
+
+        if guard is None:
+            run()
+        else:
+            pl.when(guard)(run)
+
+    def to_peer(i, src, dst):
+        return pltpu.make_async_remote_copy(
+            src_ref=src, dst_ref=dst, send_sem=tp_send.at[i], recv_sem=tp_recv.at[i],
+            device_id={"tp": peer}, device_id_type=MESH,
+        )
+
+    tok_copy = to_peer(0, tokens, tok_peer)
+    tok_copy.start()
+    stat_copy = to_peer(1, stat, stat_peer)
+    part_copy = to_peer(2, part_send, part_recv)
+    mid_copy = to_peer(3, middle, mid_peer)
+    down_copy = to_peer(4, down_send, down_recv)
+
+    def norm_rows(mine, other, gain):
+        def block(r, carry):
+            at_rows = pl.ds(pl.multiple_of(r * 32, 32), 32)
+            a = mine[at_rows, :].astype(jnp.float32)
+            b = other[at_rows, :].astype(jnp.float32)
+            total = jnp.sum(a * a, axis=-1, keepdims=True) + jnp.sum(b * b, axis=-1, keepdims=True)
+            scale = lax.rsqrt(total / width + EPS)
+            normed[core, at_rows, :] = (a * scale * gain[core]).astype(jnp.bfloat16)
+            normed[peer, at_rows, :] = (b * scale * gain[peer]).astype(jnp.bfloat16)
+            return carry
+
+        lax.fori_loop(0, tok_rows // 32, block, 0)
+
+    def project(name, cols):
+        total = None
+        for h in (0, 1):
+            weight = held[name][h * half:(h + 1) * half, :, :, :, cols]
+            weight = weight.reshape(-1, weight.shape[-1])
+            term = jnp.dot(normed[h], weight, preferred_element_type=jnp.float32)
+            total = term if total is None else total + term
+        return total
+
+    def project_back(left, name, side):
+        weight = held[name][pl.ds(side * half, half)]
+        weight = weight.reshape(-1, weight.shape[-1])
+        return lax.dot_general(left, weight, (((1,), (1,)), ((), ())), preferred_element_type=jnp.float32)
+
+    def norm1():
+        tok_copy.wait_recv()
+        pad[...] = jnp.zeros_like(pad)
+        norm_rows(tokens, tok_peer, gain1)
+
+    def mixv():
+        for c in range(0, mix_cols, 256):
+            mvbuf[:, c:c + 256] = project("mv", slice(c, c + 256))
+
+    seqs = tok_rows // SEQ_LEN
+    lead = -(-(taps // 2) // 8) * 8
+
+    def mixg():
+        for c in range(0, mix_cols, 256):
+            glu = mvbuf[:, c:c + 256] * jax.nn.sigmoid(project("mg", slice(c, c + 256)))
+            pad[:, lead:lead + SEQ_LEN, c:c + 256] = glu.reshape(seqs, SEQ_LEN, 256)
+
+    def conv(lo, hi):
+        def block(i, carry):
+            s, c = lax.div(i, hi - lo), lo + lax.rem(i, hi - lo)
+            lanes = pl.ds(pl.multiple_of(c * 128, 128), 128)
+            total = jnp.zeros((SEQ_LEN, 128), jnp.float32)
+            for k in range(taps):
+                total = total + pad[s, pl.ds(lead - taps // 2 + k, SEQ_LEN), lanes] * kern[k:k + 1, lanes]
+            mixed[pl.ds(pl.multiple_of(s * SEQ_LEN, SEQ_LEN), SEQ_LEN), lanes] = total
+            return carry
+
+        lax.fori_loop(0, seqs * (hi - lo), block, 0)
+
+    lane_blocks = mix_cols // 128
+
+    def stats():
+        def block(r, carry):
+            at_rows = pl.ds(pl.multiple_of(r * 64, 64), 64)
+            v = mixed[at_rows, :]
+            first = jnp.sum(v, axis=-1, keepdims=True)
+            second = jnp.sum(v * v, axis=-1, keepdims=True)
+            lane = lax.broadcasted_iota(jnp.int32, (64, 128), 1)
+            stat[at_rows, :] = jnp.where(lane == 0, first, second)
+            return carry
+
+        lax.fori_loop(0, tok_rows // 64, block, 0)
+        stat_copy.start()
+
+    def make_active():
+        stat_copy.wait_recv()
+
+        def block(r, carry):
+            at_rows = pl.ds(pl.multiple_of(r * 32, 32), 32)
+            both = stat[at_rows, :] + stat_peer[at_rows, :]
+            mean = both[:, 0:1] / (2 * mix_cols)
+            var = jnp.maximum(both[:, 1:2] / (2 * mix_cols) - mean * mean, 0.0)
+            v = (mixed[at_rows, :] - mean) * lax.rsqrt(var + EPS) * cgain[...] + cbias[...]
+            active[at_rows, :] = (v * jax.nn.sigmoid(v)).astype(jnp.bfloat16)
+            return carry
+
+        lax.fori_loop(0, tok_rows // 32, block, 0)
+
+    def out_peer():
+        part_send[...] = project_back(active[...], "mo", peer)
+        part_copy.start()
+
+    def out_mine():
+        part_mine[...] = project_back(active[...], "mo", core)
+
+    def make_middle():
+        part_copy.wait_recv()
+        middle[...] = (tokens[...].astype(jnp.float32) + (part_mine[...] + part_recv[...])).astype(jnp.bfloat16)
+        mid_copy.start()
+
+    def norm2():
+        mid_copy.wait_recv()
+        norm_rows(middle, mid_peer, gain2)
+
+    def short_conv(values, kernel_rows):
+        pos = lax.rem(lax.broadcasted_iota(jnp.int32, values.shape, 0), SEQ_LEN)
+        total = None
+        for k in range(ffn_taps):
+            shift = k - ffn_taps // 2
+            term = values
+            if shift:
+                term = pltpu.roll(values, (-shift) % tok_rows, 0)
+                inside = pos < SEQ_LEN - shift if shift > 0 else pos >= -shift
+                term = jnp.where(inside, term, 0.0)
+            term = term * kernel_rows[k:k + 1, :]
+            total = term if total is None else total + term
+        return total
+
+    first = cols_of["v0"]
+
+    def up(g):
+        count = hidden[g].shape[1]
+        for c in range(0, count, 256):
+            at_cols = slice(g * first + c, g * first + c + 256)
+            if g < 2:
+                value = project("v%d" % g, slice(c, c + 256))
+                gate = project("g%d" % g, slice(c, c + 256))
+            else:
+                value = project("vg2", slice(c, c + 256))
+                gate = project("vg2", slice(count + c, count + c + 256))
+            value = short_conv(value, vkern[:, at_cols])
+            gate = short_conv(gate, gkern[:, at_cols])
+            hidden[g][:, c:c + 256] = (gate * jax.nn.sigmoid(gate) * value).astype(jnp.bfloat16)
+
+    fresh = {"peer": True, "mine": True}
+
+    def down(g, side, which, buf):
+        term = project_back(hidden[g][...], "w%d" % g, side)
+        if fresh[which]:
+            buf[...] = term
+        else:
+            buf[...] += term
+        fresh[which] = False
+
+    def finish():
+        down_copy.wait_recv()
+        total = middle[...].astype(jnp.float32) + (down_mine[...] + down_recv[...])
+        out[...] = total.astype(jnp.bfloat16)
+
+    run = {
+        "norm1": norm1, "mixv": mixv, "mixg": mixg,
+        "conv_a": lambda: conv(0, lane_blocks // 2),
+        "conv_b": lambda: conv(lane_blocks // 2, lane_blocks),
+        "stats": stats, "active": make_active, "out_peer": out_peer, "out_mine": out_mine,
+        "middle": make_middle, "norm2": norm2, "send_down": lambda: down_copy.start(), "finish": finish,
+    }
+    for g in (0, 1, 2):
+        run["up%d" % g] = functools.partial(up, g)
+        run["down_peer%d" % g] = functools.partial(down, g, peer, "peer", down_send)
+        run["down_mine%d" % g] = functools.partial(down, g, core, "mine", down_mine)
+
+    for kind, key in program:
+        if kind == "send":
+            act(key, True, lambda copy: copy.start())
+        elif kind == "recv":
+            act(key, False, lambda copy: copy.wait_recv())
+        elif kind == "local":
+            for copy in local:
+                copy.wait()
+        else:
+            run[key]()
+    for key in transfers:
+        act(key, True, lambda copy: copy.wait_send())
+    for copy in (tok_copy, stat_copy, part_copy, mid_copy, down_copy):
+        copy.wait_send()
+
+
+def fused_body(fs_size, tokens, mix_gain, mix_value_w, mix_gate_w, mix_kernel, chan_gain, chan_bias, mix_out_w,
+               ffn_gain, ffn_value_w, ffn_gate_w, ffn_value_kernel, ffn_gate_kernel, ffn_down_w):
+    rows, mix_cols = mix_value_w.shape
+    ffn_cols = ffn_value_w.shape[1]
+    tok_rows, tok_cols = tokens.shape
+    line = fs_size // 4
+    plan, gates = chunk_plan(mix_cols, ffn_cols)
+    transfers = build_transfers(plan, gates, line)
+    program = order_events(transfers, compute_list(3))
+    first = [item[2] for item in plan if item[0] == "v0"][0]
+    rest = ffn_cols - 2 * first
+    v, g, w = ffn_value_w, ffn_gate_w, ffn_down_w.T
+    pieces = {
+        "mv": [mix_value_w], "mg": [mix_gate_w], "mo": [mix_out_w.T],
+        "v0": [v[:, :first]], "v1": [v[:, first:2 * first]],
+        "g0": [g[:, :first]], "g1": [g[:, first:2 * first]],
+        "w0": [w[:, :first]], "w1": [w[:, first:2 * first]], "w2": [w[:, 2 * first:]],
+        "vg2": [v[:, 2 * first:], g[:, 2 * first:]],
+    }
+    packed = jnp.concatenate(
+        [part.astype(jnp.bfloat16) for item in plan for part in pieces[item[0]]], axis=1
+    )
+    sizes = (line, rows, tok_rows, mix_cols, ffn_cols, 2 * tok_cols, mix_kernel.shape[0], ffn_value_kernel.shape[0])
+    vm = pltpu.VMEM
+    f32, bf16 = jnp.float32, jnp.bfloat16
+    lead = -(-(mix_kernel.shape[0] // 2) // 8) * 8
+    seqs = tok_rows // SEQ_LEN
+    full = (tok_rows, tok_cols)
+    scratch = [vm((line, 2, 2, rows, item[2]), bf16) for item in plan] + [
+        vm(full, bf16), vm((2,) + full, bf16), vm((tok_rows, mix_cols), f32),
+        vm((seqs, SEQ_LEN + 2 * lead, mix_cols), f32), vm((tok_rows, mix_cols), f32),
+        vm((tok_rows, 128), f32), vm((tok_rows, 128), f32), vm((tok_rows, mix_cols), bf16),
+        vm(full, f32), vm(full, f32), vm(full, f32), vm(full, bf16), vm(full, bf16),
+        vm((tok_rows, first), bf16), vm((tok_rows, first), bf16), vm((tok_rows, rest), bf16),
+        vm(full, f32), vm(full, f32), vm(full, f32),
+        pltpu.SemaphoreType.DMA((len(transfers),)), pltpu.SemaphoreType.DMA((len(transfers),)),
+        pltpu.SemaphoreType.DMA((len(plan),)), pltpu.SemaphoreType.DMA((5,)), pltpu.SemaphoreType.DMA((5,)),
+    ]
+    return pl.pallas_call(
+        functools.partial(layer_kernel, sizes, plan, transfers, program),
+        out_shape=jax.ShapeDtypeStruct(full, bf16),
+        in_specs=[pl.BlockSpec(memory_space=vm)] * 9,
+        out_specs=pl.BlockSpec(memory_space=vm),
+        scratch_shapes=scratch,
+        compiler_params=pltpu.CompilerParams(
+            collective_id=0, has_side_effects=True, vmem_limit_bytes=56 * 1024 * 1024
+        ),
+    )(
+        tokens, mix_gain.reshape(2, 1, tok_cols), mix_kernel, chan_gain.reshape(1, -1), chan_bias.reshape(1, -1),
+        ffn_gain.reshape(2, 1, tok_cols), ffn_value_kernel, ffn_gate_kernel, packed,
+    )
+
+
+def pick_body(fs_size, tp_size):
+    def run(*args):
+        tokens, mix_w, ffn_w = args[0], args[2], args[9]
+        fits = (
+            tp_size == 2 and fs_size % 8 == 0 and fs_size <= 32
+            and mix_w.shape[0] % 16 == 0 and mix_w.shape[1] % 256 == 0
+            and ffn_w.shape[1] % 256 == 0 and ffn_w.shape[1] >= 768
+            and tokens.shape[0] % 64 == 0 and tokens.shape[1] % 128 == 0
+            and fs_size * mix_w.shape[0] == tp_size * tokens.shape[1]
+            and fs_size * args[7].shape[1] == tp_size * tokens.shape[1]
+        )
+        if fits:
+            return fused_body(fs_size, *args)
+        return body(*args)
+
+    return run
+
+
 def solution(mesh):
     return jax.shard_map(
-        body,
+        pick_body(mesh.shape["fs"], mesh.shape["tp"]),
         mesh=mesh,
         in_specs=(
             P("fs", "tp"),

time: 411 us -> 109 us (0.27)
  waiting for transfers between devices: 360 us -> 0 us
  Pallas kernels: 0 us -> 101 us
  matrix products: 15.1 us -> 0 us
  between operations: 13.7 us -> 0.11 us
  other arithmetic: 13.9 us -> 1.11 us
  blocking collectives: 7.17 us -> 0 us
  local copies, waits for them, and re-layouts: 0.45 us -> 6.18 us
    all_gather x6 -> x0, waiting for transfers between devices: 347 us -> none  [the longest x2 119 us: project_in(): lax.all_gather(weight_one.astype(jnp.bfloat16), 'fs', axis=0, tiled=True)]
    pallas_call x0 -> x1, Pallas kernels: none -> 101 us  [fused_body(): pl.pallas_call(functools.partial(layer_kernel, sizes, plan, transfers, pr...]
    dot_general x6 -> x0, matrix products: 15.1 us -> none  [the longest x2 6.38 us: apply_piece(): jnp.dot(active, piece.astype(jnp.bfloat16), preferred_element_type=jnp.fl...]
    reduce_scatter x2 -> x0, waiting for transfers between devices: 12.1 us -> none  [project_out(): lax.psum_scatter(partial_terms, 'tp', scatter_dimension=1, tiled=True)]
    convert_element_type x10 -> x0, other arithmetic: 10.3 us -> none  [the longest x2 2.26 us: project_in(): weight_two.astype(jnp.bfloat16)]
    unnamed x22 -> x20, local copies, waits for them, and re-layouts: 0.15 us -> 6.18 us
    all_gather x2 -> x0, blocking collectives: 4.73 us -> none  [collect_rows(): return lax.all_gather(local_rows, 'tp', axis=1, tiled=True)]
  transfers between devices with their start and end apart: 8 -> 0, of which waited for: 8 -> 0; matrix products, arithmetic and copies ran while one was open for 5% -> 0% of each run, Pallas kernels for 0% -> 0%
where the time goes in v1:
time: 109 us
  Pallas kernels  101 us (93%)
  local copies, waits for them, and re-layouts  6.18 us (6%)
  other arithmetic  1.11 us (1%)
    pallas_call x1, Pallas kernels, fused_body(): pl.pallas_call(functools.partial(layer_kernel, sizes, plan, transfers, pr...  101 us
    unnamed x20, local copies, waits for them, and re-layouts  6.18 us

profile of v1, /device:TPU:0, one launch (start us, length us, event | category | flops | bytes accessed | tf_op | source)
XLA Modules:
  0.0 108.6 jit_solution(2644948037169154986)
XLA Ops:
  0.0 0.0 copy-start.1
  0.0 1.0 convert.15
  1.0 0.0 copy-done.1
  1.1 0.0 copy-start.2
  1.1 0.9 copy-done.2
  2.0 0.0 copy-start.3
  2.1 0.9 copy-done.3
  3.0 0.0 copy-start.4
  3.0 0.9 copy-done.4
  3.9 0.0 copy-start.5
  3.9 0.9 copy-done.5
  4.9 0.0 copy-start
  4.9 0.8 copy-done
  5.7 101.2 %shard_map.136 = bf16[256,512]{1,0:T(8,128)(2,1)} custom-call(bf16[256,512]{1,0:T(8,128)(2,1)} %refs_0_.1, f32[2,1,512]{2,1,0:T(1,128)} %bitcast.8, f32[31,512]{1,0:T(8,128)} %refs_2_.1, f32[1,512]{1,0:T(1,128)} %bitcast.10, f32[1,512]{1,0:T(1,128)} %bitcast.11, f32[2,1,512]{2,1,0:T(1,128)} %bitcast.9, f32[3,1280]{1,0:T(4,128)} %refs_6_.1, ...), custom_call_target="tpu_custom_call" | custom-call | tf_op jit(solution)/shard_map/pallas_call | solution.py:572
  106.9 1.7 %copy.26 = bf16[256,512]{1,0:T(8,128)(2,1)} copy(bf16[256,512]{1,0:T(8,128)(2,1)} %shard_map.136) | data formatting | bytes 524288
  (13 shorter events, 0.1 us)
Async XLA Ops:
  0.0 1.1 copy-start.1
  1.1 1.0 copy-start.2
  2.0 0.9 copy-start.3
  3.0 0.9 copy-start.4
  3.9 0.9 copy-start.5
  4.9 0.8 copy-start

commit v2 on v0

--- a/solution.py
+++ b/solution.py
@@ -1,6 +1,10 @@
+import functools
+
 import jax
 import jax.numpy as jnp
 from jax import lax
+from jax.experimental import pallas as pl
+from jax.experimental.pallas import tpu as pltpu
 from jax.sharding import PartitionSpec as P
 
 CONV_W = 1024
@@ -99,9 +103,535 @@
     return (middle.astype(jnp.float32) + project_out(hidden, ffn_down_w)).astype(jnp.bfloat16)
 
 
+MESH = pl.DeviceIdType.MESH
+UNIT_US = 0.36
+HOP_US = 1.8
+
+
+def chunk_plan(mix_cols, ffn_cols):
+    wide = (2 * ffn_cols // 5) // 128 * 128
+    rest = ffn_cols - 2 * wide
+    plan = [
+        ("mv", "A", mix_cols), ("mg", "A", mix_cols), ("mo", "A", mix_cols),
+        ("vg0", "A", 2 * wide), ("vg1", "A", 2 * wide), ("vg2", "A", 2 * rest),
+        ("w0", "A", wide), ("w1", "B", wide), ("w2", "B", rest),
+    ]
+    gates = {
+        "vg1": ("vg0", "u", 1), "vg2": ("vg1", "u", 1), "w0": ("vg1", "u", 2),
+        "w1": ("vg2", "u", 2), "w2": ("w0", "u", 2),
+    }
+    return plan, gates, (wide, wide, rest)
+
+
+def build_transfers(plan, gates, line):
+    out = {}
+    steps = range(1, line)
+    for name, kind, cols in plan:
+        out[(name, "1")] = dict(link="x", size=cols // 128, deps=[], phase="p1")
+    for name, kind, cols in plan:
+        width = cols // 128
+        gate = [gates[name]] if name in gates else []
+        if kind == "A":
+            for t in steps:
+                for d in "ud":
+                    deps = [(name, d, t - 1)] if t > 1 else [(name, "1")] + gate
+                    out[(name, d, t)] = dict(link="z" + d, size=2 * width, deps=deps, phase="z")
+            out[(name, "y", "o", 0)] = dict(link="y", size=2 * width, deps=[(name, "1")], phase="y")
+            for t in steps:
+                for d in "ud":
+                    out[(name, "y", d, t)] = dict(link="y", size=2 * width, deps=[(name, d, t)], phase="y")
+        else:
+            out[(name, "y", "o", 0)] = dict(link="y", size=2 * width, deps=[(name, "1")], phase="y")
+            for t in steps:
+                for d in "ud":
+                    deps = [(name, d, t - 1)] if t > 1 else [(name, "y", "o", 0)] + gate
+                    out[(name, d, t)] = dict(link="z" + d, size=4 * width, deps=deps, phase="q")
+    return out
+
+
+def order_events(transfers, computes):
+    free, arrival, seen, done = {}, {}, set(), {}
+    program, now = [], 0.0
+
+    def issue():
+        for key, item in transfers.items():
+            if key not in arrival and all(dep in seen for dep in item["deps"]):
+                start = max(now, free.get(item["link"], 0.0))
+                free[item["link"]] = start + item["size"] * UNIT_US
+                arrival[key] = free[item["link"]] + HOP_US
+                program.append(("send", key))
+                if key == ("mo", "1"):
+                    program.append(("compute", "tok_start"))
+                    free["x"] += 5.6
+
+    issue()
+    program.append(("local", None))
+    while len(seen) < len(transfers) or len(done) < len(computes):
+        events = [(arrival[key], i, key) for i, key in enumerate(transfers) if key in arrival and key not in seen]
+        ready = []
+        for i, (name, needs, after, cost, delay) in enumerate(computes):
+            if name in done or not all(a in done for a in after):
+                continue
+            if all(key in seen for key in transfers if key[0] in needs):
+                ready.append((max([delay] + [done[a] + delay for a in after]), i, name, cost))
+        can = [r for r in ready if r[0] <= now]
+        if events and min(events)[0] <= now:
+            pick = min(events)
+        elif can:
+            pick = min(can, key=lambda r: r[1])
+        else:
+            pick = min(events + ready, key=lambda r: r[0])
+            now = max(now, pick[0])
+        if len(pick) == 3:
+            seen.add(pick[2])
+            program.append(("recv", pick[2]))
+            issue()
+        else:
+            program.append(("compute", pick[2]))
+            now += pick[3]
+            done[pick[2]] = now
+    return program
+
+
+def compute_list():
+    items = [
+        ("tok_fwd", (), (), 0.2, 10.0),
+        ("norm1", (), ("tok_fwd",), 2.0, 1.5),
+        ("mixv", ("mv",), ("norm1",), 0.8, 0.0),
+        ("mixg", ("mg",), ("mixv",), 1.0, 0.0),
+        ("conv_a", (), ("mixg",), 1.2, 0.0),
+        ("conv_b", (), ("conv_a",), 1.2, 0.0),
+        ("stats", (), ("conv_b",), 0.7, 0.0),
+        ("active", (), ("stats",), 1.5, 2.5),
+        ("out_far", ("mo",), ("active",), 0.8, 0.0),
+        ("out_near", (), ("out_far",), 0.8, 0.0),
+        ("out_x", (), ("out_near",), 0.5, 0.8),
+        ("middle", (), ("out_x",), 0.8, 8.0),
+        ("mid_fwd", (), ("middle",), 0.2, 8.0),
+        ("norm2", (), ("mid_fwd",), 2.0, 1.5),
+    ]
+    for g in (0, 1, 2):
+        items.append(("up%d" % g, ("vg%d" % g,), ("norm2",), (2.0, 2.0, 1.0)[g], 0.0))
+    for g in (0, 1, 2):
+        items.append(("down_far%d" % g, ("w%d" % g,), ("up%d" % g,), 0.5, 0.0))
+    items.append(("send_far", (), tuple("down_far%d" % g for g in (0, 1, 2)), 0.1, 0.0))
+    for g in (0, 1, 2):
+        items.append(("down_near%d" % g, (), ("send_far", ), 0.5, 0.0))
+    items.append(("down_x", (), tuple("down_near%d" % g for g in (0, 1, 2)), 0.5, 0.0))
+    items.append(("finish", (), ("down_x",), 1.0, 7.5))
+    return items
+
+
+def layer_kernel(sizes, plan, groups, transfers, program, *refs):
+    line, tok_rows, tok_cols, mix_cols, ffn_cols, taps, ffn_taps, total_cols = sizes
+    (tokens, gain1, kern, cgain, cbias, gain2, vkern, gkern, packed) = refs[:9]
+    out = refs[9]
+    scratch = refs[10:]
+    held = {item[0]: scratch[i] for i, item in enumerate(plan)}
+    (tokall, midall, normed, mvbuf, pad, mixed, stat, stats_in, active,
+     far_peer, far_mine, far_in, near_peer, near_mine, near_in, x_out, x_in,
+     hid0, hid1, hid2, down_far_peer, down_far_mine, down_far_in,
+     down_near_peer, down_near_mine, down_near_in, down_x_out, down_x_in,
+     send_sem, recv_sem, loc_sem, act_send, act_recv) = scratch[len(plan):]
+    hidden = (hid0, hid1, hid2)
+    width = 2 * tok_cols
+    offsets, at = {}, 0
+    for name, _, cols in plan:
+        offsets[name] = at
+        at += cols
+    cols_of = {item[0]: item[2] for item in plan}
+    numbers = {key: i for i, key in enumerate(transfers)}
+    fs = lax.axis_index("fs")
+    core = lax.axis_index("tp")
+    peer = 1 - core
+    z, y, x = lax.div(fs, 4), lax.rem(lax.div(fs, 2), 2), lax.rem(fs, 2)
+    far = 1 - x
+    at_y, at_x = fs + 2 - 4 * y, fs + 1 - 2 * x
+    half = line // 2
+
+    barrier = pltpu.get_barrier_semaphore()
+    for dev in ({"fs": at_y}, {"fs": at_x}, {"tp": peer}, {"fs": at_x, "tp": peer}):
+        pl.semaphore_signal(barrier, inc=1, device_id=dev, device_id_type=MESH)
+
+    @pl.when(z > 0)
+    def _():
+        pl.semaphore_signal(barrier, inc=1, device_id={"fs": fs - 4}, device_id_type=MESH)
+
+    @pl.when(z < line - 1)
+    def _():
+        pl.semaphore_signal(barrier, inc=1, device_id={"fs": fs + 4}, device_id_type=MESH)
+
+    def piece(name, part):
+        lanes = pl.ds(pl.multiple_of(part * total_cols + offsets[name], 128), cols_of[name])
+        return packed.at[:, lanes]
+
+    local = []
+    for i, (name, _, cols) in enumerate(plan):
+        local.append(pltpu.make_async_copy(piece(name, x), held[name].at[z, y, x], loc_sem.at[i]))
+    local.append(pltpu.make_async_copy(tokens, tokall.at[x, core], loc_sem.at[len(plan)]))
+    for copy in local:
+        copy.start()
+    pl.semaphore_wait(barrier, 4 + jnp.minimum(z, 1) + jnp.minimum(line - 1 - z, 1))
+
+    def guards(key, sending):
+        phase = transfers[key]["phase"]
+        if phase in ("z", "q"):
+            d, t = key[1], key[2]
+            if d == "u":
+                return jnp.logical_and(z >= t - 1, z < line - 1) if sending else z >= t
+            return jnp.logical_and(z <= line - t, z > 0) if sending else z <= line - 1 - t
+        if phase == "y" and key[2] != "o":
+            d, t = key[2], key[3]
+            return z >= t if d == "u" else z <= line - 1 - t
+        return None
+
+    def make(key, sending):
+        phase, name, i = transfers[key]["phase"], key[0], numbers[key]
+        buf = held[name]
+        src = None
+        if phase in ("z", "q"):
+            d, t = key[1], key[2]
+            back = t - 1 if sending else t
+            block = z - back if d == "u" else z + back
+            dev = {"fs": fs + 4 if d == "u" else fs - 4}
+            dst = buf.at[block, y] if phase == "z" else buf.at[block]
+        elif phase == "y":
+            d, t = key[2], key[3]
+            block = z + t if d == "d" else z - t
+            dev = {"fs": at_y}
+            dst = buf.at[block, y if sending else 1 - y]
+        else:
+            dev = {"fs": at_x}
+            dst = buf.at[z, y, x if sending else far]
+            if sending:
+                src = piece(name, far)
+        return pltpu.make_async_remote_copy(
+            src_ref=dst if src is None else src, dst_ref=dst, send_sem=send_sem.at[i],
+            recv_sem=recv_sem.at[i], device_id=dev, device_id_type=MESH,
+        )
+
+    def act(key, sending, what):
+        guard = guards(key, sending)
+
+        def run():
+            what(make(key, sending))
+
+        if guard is None:
+            run()
+        else:
+            pl.when(guard)(run)
+
+    acts = []
+
+    def exchange(src, dst, landed, **dev):
+        i = len(acts)
+        acts.append(None)
+
+        def build(s, d):
+            return pltpu.make_async_remote_copy(
+                src_ref=s, dst_ref=d, send_sem=act_send.at[i], recv_sem=act_recv.at[i],
+                device_id=dev, device_id_type=MESH,
+            )
+
+        acts[i] = build(src, dst)
+        return build(src, dst).start, build(landed, landed).wait_recv
+
+    tok_core = exchange(tokens, tokall.at[x, core], tokall.at[x, peer], tp=peer)
+    tok_x = exchange(tokens, tokall.at[x, core], tokall.at[far, core], fs=at_x)
+    tok_fwd = exchange(tokall.at[far, core], tokall.at[far, core], tokall.at[far, peer], tp=peer)
+    mid_core = exchange(midall.at[x, core], midall.at[x, core], midall.at[x, peer], tp=peer)
+    mid_x = exchange(midall.at[x, core], midall.at[x, core], midall.at[far, core], fs=at_x)
+    mid_fwd = exchange(midall.at[far, core], midall.at[far, core], midall.at[far, peer], tp=peer)
+    stat_all = [
+        exchange(stat, stats_in.at[0], stats_in.at[0], tp=peer),
+        exchange(stat, stats_in.at[1], stats_in.at[1], fs=at_x),
+        exchange(stat, stats_in.at[2], stats_in.at[2], fs=at_x, tp=peer),
+    ]
+    out_far = exchange(far_peer, far_in, far_in, tp=peer)
+    out_near = exchange(near_peer, near_in, near_in, tp=peer)
+    out_x = exchange(x_out, x_in, x_in, fs=at_x)
+    down_far = exchange(down_far_peer, down_far_in, down_far_in, tp=peer)
+    down_near = exchange(down_near_peer, down_near_in, down_near_in, tp=peer)
+    down_x = exchange(down_x_out, down_x_in, down_x_in, fs=at_x)
+
+    def norm_rows(rows_of, gain):
+        for side in (0, 1):
+            def block(r, carry):
+                at_rows = pl.ds(pl.multiple_of(r * 32, 32), 32)
+                a = rows_of[side, 0, at_rows, :].astype(jnp.float32)
+                b = rows_of[side, 1, at_rows, :].astype(jnp.float32)
+                total = jnp.sum(a * a + b * b, axis=-1, keepdims=True)
+                scale = lax.rsqrt(total / width + EPS)
+                normed[0, side, at_rows, :] = (a * scale * gain[0]).astype(jnp.bfloat16)
+                normed[1, side, at_rows, :] = (b * scale * gain[1]).astype(jnp.bfloat16)
+                return carry
+
+            lax.fori_loop(0, tok_rows // 32, block, 0)
+
+    def project(name, lo, hi):
+        total = None
+        for h in (0, 1):
+            weight = held[name][h * half:(h + 1) * half, :, :, :, lo:hi]
+            weight = weight.reshape(-1, hi - lo)
+            left = normed[h].reshape(2 * tok_rows, tok_cols)
+            term = jnp.dot(left, weight, preferred_element_type=jnp.float32)
+            total = term if total is None else total + term
+        return total
+
+    def project_back(left, name, side):
+        weight = held[name][pl.ds(side * half, half)]
+        weight = weight.reshape(-1, weight.shape[-1])
+        return lax.dot_general(left, weight, (((1,), (1,)), ((), ())), preferred_element_type=jnp.float32)
+
+    def start_tokens():
+        tok_core[0]()
+        tok_x[0]()
+
+    def forward_tokens():
+        tok_x[1]()
+        tok_fwd[0]()
+
+    def norm1():
+        pad[...] = jnp.zeros_like(pad)
+        tok_core[1]()
+        tok_fwd[1]()
+        norm_rows(tokall, gain1)
+
+    seqs = 2 * tok_rows // SEQ_LEN
+    lead = -(-(taps // 2) // 8) * 8
+
+    def mixv():
+        mvbuf[...] = project("mv", 0, mix_cols)
+
+    def mixg():
+        glu = mvbuf[...] * jax.nn.sigmoid(project("mg", 0, mix_cols))
+        pad[:, lead:lead + SEQ_LEN, :] = glu.reshape(seqs, SEQ_LEN, mix_cols)
+
+    lane_blocks = mix_cols // 128
+
+    def conv(lo, hi):
+        def block(i, carry):
+            s, c = lo + lax.div(i, lane_blocks), lax.rem(i, lane_blocks)
+            lanes = pl.ds(pl.multiple_of(c * 128, 128), 128)
+            taps_at = pl.ds(pl.multiple_of(x * mix_cols + c * 128, 128), 128)
+            total = jnp.zeros((SEQ_LEN, 128), jnp.float32)
+            for k in range(taps):
+                total = total + pad[s, pl.ds(lead - taps // 2 + k, SEQ_LEN), lanes] * kern[k:k + 1, taps_at]
+            mixed[pl.ds(pl.multiple_of(s * SEQ_LEN, SEQ_LEN), SEQ_LEN), lanes] = total
+            return carry
+
+        lax.fori_loop(0, (hi - lo) * lane_blocks, block, 0)
+
+    def stats():
+        for r in range(0, 2 * tok_rows, 128):
+            v = mixed[r:r + 128, :]
+            first = jnp.sum(v, axis=-1, keepdims=True)
+            second = jnp.sum(v * v, axis=-1, keepdims=True)
+            lane = lax.broadcasted_iota(jnp.int32, (128, 128), 1)
+            stat[:, r:r + 128] = jnp.where(lane == 0, first, second).T[:8]
+        for send, _ in stat_all:
+            send()
+
+    def make_active():
+        for _, wait in stat_all:
+            wait()
+        for r in range(0, 2 * tok_rows, 128):
+            both = stat[:, r:r + 128] + stats_in[0, :, r:r + 128] + (
+                stats_in[1, :, r:r + 128] + stats_in[2, :, r:r + 128]
+            )
+            both = jnp.concatenate([both] * 16, axis=0).T
+            mean = both[:, 0:1] / (4 * mix_cols)
+            var = jnp.maximum(both[:, 1:2] / (4 * mix_cols) - mean * mean, 0.0)
+            v = (mixed[r:r + 128, :] - mean) * lax.rsqrt(var + EPS) * cgain[x] + cbias[x]
+            active[r:r + 128, :] = (v * jax.nn.sigmoid(v)).astype(jnp.bfloat16)
+
+    def rows_at(side):
+        return pl.ds(pl.multiple_of(side * tok_rows, tok_rows), tok_rows)
+
+    def make_out_far():
+        left = active[rows_at(far), :]
+        far_peer[...] = project_back(left, "mo", peer)
+        out_far[0]()
+        far_mine[...] = project_back(left, "mo", core)
+
+    def make_out_near():
+        left = active[rows_at(x), :]
+        near_peer[...] = project_back(left, "mo", peer)
+        out_far[1]()
+        x_out[...] = (far_mine[...] + far_in[...]).astype(jnp.bfloat16)
+        out_x[0]()
+        out_near[0]()
+        near_mine[...] = project_back(left, "mo", core)
+
+    def make_out_x():
+        out_near[1]()
+        near_mine[...] += near_in[...]
+
+    def make_middle():
+        out_x[1]()
+        total = tokens[...].astype(jnp.float32) + (near_mine[...] + x_in[...].astype(jnp.float32))
+        midall[x, core] = total.astype(jnp.bfloat16)
+        mid_x[0]()
+        mid_core[0]()
+
+    def forward_middle():
+        mid_x[1]()
+        mid_fwd[0]()
+
+    def norm2():
+        mid_core[1]()
+        mid_fwd[1]()
+        norm_rows(midall, gain2)
+
+    def short_conv(values, kernel_rows, lanes):
+        pos = lax.rem(lax.broadcasted_iota(jnp.int32, values.shape, 0), SEQ_LEN)
+        total = None
+        for k in range(ffn_taps):
+            shift = k - ffn_taps // 2
+            term = values
+            if shift:
+                term = pltpu.roll(values, (-shift) % (2 * tok_rows), 0)
+                inside = pos < SEQ_LEN - shift if shift > 0 else pos >= -shift
+                term = jnp.where(inside, term, 0.0)
+            term = term * kernel_rows[k:k + 1, lanes]
+            total = term if total is None else total + term
+        return total
+
+    def up(g):
+        count = groups[g]
+        start = sum(groups[:g])
+        for c in range(0, count, 256):
+            n = min(256, count - c)
+            lanes = pl.ds(pl.multiple_of(x * ffn_cols + start + c, 128), n)
+            name = "vg%d" % g
+            value = short_conv(project(name, c, c + n), vkern, lanes)
+            gate = short_conv(project(name, count + c, count + c + n), gkern, lanes)
+            hidden[g][:, c:c + n] = (gate * jax.nn.sigmoid(gate) * value).astype(jnp.bfloat16)
+
+    fresh = set()
+
+    def down(g, where, name, peer_buf, mine_buf):
+        left = hidden[g][rows_at(where), :]
+        for side, buf in ((peer, peer_buf), (core, mine_buf)):
+            term = project_back(left, "w%d" % g, side)
+            if name in fresh:
+                buf[...] += term
+            else:
+                buf[...] = term
+        fresh.add(name)
+
+    def make_down_x():
+        down_near[0]()
+        down_far[1]()
+        down_x_out[...] = (down_far_mine[...] + down_far_in[...]).astype(jnp.bfloat16)
+        down_x[0]()
+
+    def finish():
+        down_near[1]()
+        near = down_near_mine[...] + down_near_in[...] + midall[x, core].astype(jnp.float32)
+        down_near_mine[...] = near
+        down_x[1]()
+        out[...] = (down_near_mine[...] + down_x_in[...].astype(jnp.float32)).astype(jnp.bfloat16)
+
+    run = {
+        "tok_start": start_tokens, "tok_fwd": forward_tokens, "norm1": norm1, "mixv": mixv, "mixg": mixg,
+        "conv_a": lambda: conv(0, seqs // 2), "conv_b": lambda: conv(seqs // 2, seqs),
+        "stats": stats, "active": make_active, "out_far": make_out_far, "out_near": make_out_near,
+        "out_x": make_out_x, "middle": make_middle, "mid_fwd": forward_middle, "norm2": norm2,
+        "send_far": down_far[0], "down_x": make_down_x, "finish": finish,
+    }
+    for g in (0, 1, 2):
+        run["up%d" % g] = functools.partial(up, g)
+        run["down_far%d" % g] = functools.partial(down, g, far, "far", down_far_peer, down_far_mine)
+        run["down_near%d" % g] = functools.partial(down, g, x, "near", down_near_peer, down_near_mine)
+
+    for kind, key in program:
+        if kind == "send":
+            act(key, True, lambda copy: copy.start())
+        elif kind == "recv":
+            act(key, False, lambda copy: copy.wait_recv())
+        elif kind == "local":
+            for copy in local:
+                copy.wait()
+        else:
+            run[key]()
+    for key in transfers:
+        act(key, True, lambda copy: copy.wait_send())
+    for copy in acts:
+        copy.wait_send()
+
+
+def fused_body(fs_size, tokens, mix_gain, mix_value_w, mix_gate_w, mix_kernel, chan_gain, chan_bias, mix_out_w,
+               ffn_gain, ffn_value_w, ffn_gate_w, ffn_value_kernel, ffn_gate_kernel, ffn_down_w):
+    rows, mix_cols = mix_value_w.shape[0], mix_value_w.shape[1] // 2
+    ffn_cols = ffn_value_w.shape[1] // 2
+    tok_rows, tok_cols = tokens.shape
+    line = fs_size // 4
+    plan, gates, groups = chunk_plan(mix_cols, ffn_cols)
+    transfers = build_transfers(plan, gates, line)
+    program = order_events(transfers, compute_list())
+    bf16, f32 = jnp.bfloat16, jnp.float32
+    parts = []
+    for q in (0, 1):
+        for weight in (mix_value_w, mix_gate_w, mix_out_w.T):
+            parts.append(weight[:, q * mix_cols:(q + 1) * mix_cols])
+        cuts = [q * ffn_cols + sum(groups[:g]) for g in (0, 1, 2)]
+        for g in (0, 1, 2):
+            for weight in (ffn_value_w, ffn_gate_w):
+                parts.append(weight[:, cuts[g]:cuts[g] + groups[g]])
+        parts.append(ffn_down_w.T[:, q * ffn_cols:(q + 1) * ffn_cols])
+    packed = jnp.concatenate([part.astype(bf16) for part in parts], axis=1)
+    sizes = (line, tok_rows, tok_cols, mix_cols, ffn_cols, mix_kernel.shape[0], ffn_value_kernel.shape[0],
+             packed.shape[1] // 2)
+    vm = pltpu.VMEM
+    lead = -(-(mix_kernel.shape[0] // 2) // 8) * 8
+    both = 2 * tok_rows
+    full = (tok_rows, tok_cols)
+    sums = [vm(full, f32)] * 6 + [vm(full, bf16)] * 2
+    scratch = [vm((line, 2, 2, rows, item[2]), bf16) for item in plan] + [
+        vm((2, 2) + full, bf16), vm((2, 2) + full, bf16), vm((2, 2) + full, bf16),
+        vm((both, mix_cols), f32), vm((both // SEQ_LEN, SEQ_LEN + 2 * lead, mix_cols), f32),
+        vm((both, mix_cols), f32), vm((8, both), f32), vm((3, 8, both), f32), vm((both, mix_cols), bf16),
+    ] + sums + [vm((both, g), bf16) for g in groups] + sums + [
+        pltpu.SemaphoreType.DMA((len(transfers),)), pltpu.SemaphoreType.DMA((len(transfers),)),
+        pltpu.SemaphoreType.DMA((len(plan) + 1,)), pltpu.SemaphoreType.DMA((15,)), pltpu.SemaphoreType.DMA((15,)),
+    ]
+    return pl.pallas_call(
+        functools.partial(layer_kernel, sizes, plan, groups, transfers, program),
+        out_shape=jax.ShapeDtypeStruct(full, bf16),
+        in_specs=[pl.BlockSpec(memory_space=vm)] * 9,
+        out_specs=pl.BlockSpec(memory_space=vm),
+        scratch_shapes=scratch,
+        compiler_params=pltpu.CompilerParams(
+            collective_id=0, has_side_effects=True, vmem_limit_bytes=56 * 1024 * 1024
+        ),
+    )(
+        tokens, mix_gain.reshape(2, 1, tok_cols), mix_kernel, chan_gain.reshape(2, 1, -1),
+        chan_bias.reshape(2, 1, -1), ffn_gain.reshape(2, 1, tok_cols), ffn_value_kernel, ffn_gate_kernel, packed,
+    )
+
+
+def pick_body(fs_size, tp_size):
+    def run(*args):
+        tokens, mix_w, ffn_w = args[0], args[2], args[9]
+        fits = (
+            tp_size == 2 and fs_size % 8 == 0 and fs_size <= 32
+            and mix_w.shape[0] % 16 == 0 and mix_w.shape[1] % 256 == 0
+            and ffn_w.shape[1] % 256 == 0 and ffn_w.shape[1] >= 1024
+            and tokens.shape[0] % 64 == 0 and tokens.shape[1] % 128 == 0
+            and fs_size * mix_w.shape[0] == tp_size * tokens.shape[1]
+            and fs_size * args[7].shape[1] == tp_size * tokens.shape[1]
+        )
+        if fits:
+            return fused_body(fs_size, *args)
+        return body(*args)
+
+    return run
+
+
 def solution(mesh):
     return jax.shard_map(
-        body,
+        pick_body(mesh.shape["fs"], mesh.shape["tp"]),
         mesh=mesh,
         in_specs=(
             P("fs", "tp"),

time: 411 us -> 103 us (0.25)
  waiting for transfers between devices: 360 us -> 0 us
  Pallas kernels: 0 us -> 96.4 us
  matrix products: 15.1 us -> 0 us
  between operations: 13.7 us -> 0.2 us
  other arithmetic: 13.9 us -> 2.9 us
  blocking collectives: 7.17 us -> 0 us
    all_gather x6 -> x0, waiting for transfers between devices: 347 us -> none  [the longest x2 119 us: project_in(): lax.all_gather(weight_one.astype(jnp.bfloat16), 'fs', axis=0, tiled=True)]
    pallas_call x0 -> x1, Pallas kernels: none -> 96.4 us  [fused_body(): pl.pallas_call(functools.partial(layer_kernel, sizes, plan, groups, trans...]
    dot_general x6 -> x0, matrix products: 15.1 us -> none  [the longest x2 6.38 us: apply_piece(): jnp.dot(active, piece.astype(jnp.bfloat16), preferred_element_type=jnp.fl...]
    reduce_scatter x2 -> x0, waiting for transfers between devices: 12.1 us -> none  [project_out(): lax.psum_scatter(partial_terms, 'tp', scatter_dimension=1, tiled=True)]
    convert_element_type x10 -> x0, other arithmetic: 10.3 us -> none  [the longest x2 2.26 us: project_in(): weight_two.astype(jnp.bfloat16)]
    all_gather x2 -> x0, blocking collectives: 4.73 us -> none  [collect_rows(): return lax.all_gather(local_rows, 'tp', axis=1, tiled=True)]
  transfers between devices with their start and end apart: 8 -> 0, of which waited for: 8 -> 0; matrix products, arithmetic and copies ran while one was open for 5% -> 0% of each run, Pallas kernels for 0% -> 0%
where the time goes in v2:
time: 103 us
  Pallas kernels  96.4 us (94%)
  local copies, waits for them, and re-layouts  3.64 us (4%)
  other arithmetic  2.9 us (3%)
    pallas_call x1, Pallas kernels, fused_body(): pl.pallas_call(functools.partial(layer_kernel, sizes, plan, groups, trans...  96.4 us
    unnamed x28, local copies, waits for them, and re-layouts  3.62 us
    another operation x6, other arithmetic  2.9 us

profile of v2, /device:TPU:0, one launch (start us, length us, event | category | flops | bytes accessed | tf_op | source)
XLA Modules:
  0.0 103.1 jit_solution(1267509969054465806)
XLA Ops:
  0.0 0.0 copy-start.1
  0.0 1.0 convert.32
  1.0 0.9 convert.33
  1.9 0.0 copy-start.2
  1.9 1.0 convert_bitcast_fusion.1
  2.9 0.0 copy-done.1
  2.9 0.0 copy-done.2
  2.9 0.0 copy-start.3
  3.0 0.9 copy-done.3
  4.2 0.0 copy-start
  4.2 0.8 copy-done
  5.1 96.4 %shard_map.136 = bf16[256,512]{1,0:T(8,128)(2,1)} custom-call(bf16[256,512]{1,0:T(8,128)(2,1)} %refs_0_.1, f32[2,1,512]{2,1,0:T(1,128)} %bitcast.8, f32[31,512]{1,0:T(8,128)} %refs_2_.1, f32[2,1,256]{2,1,0:T(1,128)} %bitcast.10, f32[2,1,256]{2,1,0:T(1,128)} %bitcast.11, f32[2,1,512]{2,1,0:T(1,128)} %bitcast.9, f32[3,1280]{1,0:T(4,128)} %refs_6_.1, ...), custom_call_target="tpu_custom_call" | custom-call | tf_op jit(solution)/shard_map/pallas_call | solution.py:599
  101.4 1.7 %copy.35 = bf16[256,512]{1,0:T(8,128)(2,1)} copy(bf16[256,512]{1,0:T(8,128)(2,1)} %shard_map.136) | data formatting | bytes 524288
  (23 shorter events, 0.2 us)
Async XLA Ops:
  0.0 2.9 %copy-start.1 = (f32[64,1280]{1,0:T(8,128)S(1)}, f32[64,1280]{1,0:T(8,128)}, u32[]{:S(2)}) copy-start(f32[64,1280]{1,0:T(8,128)} %param.23) | copy-start | bytes 983044
  1.9 1.0 %copy-start.2 = (f32[64,1280]{1,0:T(8,128)S(1)}, f32[64,1280]{1,0:T(8,128)}, u32[]{:S(2)}) copy-start(f32[64,1280]{1,0:T(8,128)} %param.24) | copy-start | bytes 983044
  2.9 1.0 copy-start.3
  4.2 0.9 copy-start

commit v3 on v2

--- a/solution.py
+++ b/solution.py
@@ -105,20 +105,20 @@
 
 MESH = pl.DeviceIdType.MESH
 UNIT_US = 0.36
-HOP_US = 1.8
+HOP_US = 2.2
 
 
 def chunk_plan(mix_cols, ffn_cols):
     wide = (2 * ffn_cols // 5) // 128 * 128
     rest = ffn_cols - 2 * wide
     plan = [
-        ("mv", "A", mix_cols), ("mg", "A", mix_cols), ("mo", "A", mix_cols),
+        ("mv", "A", mix_cols), ("mg", "A", mix_cols), ("mo", "B", mix_cols),
         ("vg0", "A", 2 * wide), ("vg1", "A", 2 * wide), ("vg2", "A", 2 * rest),
-        ("w0", "A", wide), ("w1", "B", wide), ("w2", "B", rest),
+        ("w0", "A", wide), ("w1", "A", wide), ("w2", "B", rest),
     ]
     gates = {
-        "vg1": ("vg0", "u", 1), "vg2": ("vg1", "u", 1), "w0": ("vg1", "u", 2),
-        "w1": ("vg2", "u", 2), "w2": ("w0", "u", 2),
+        "vg0": ("mo", "u", 1), "vg1": ("vg0", "u", 1), "vg2": ("vg1", "u", 1), "w0": ("vg2", "u", 1),
+        "w1": ("w0", "u", 1), "w2": ("w1", "u", 1),
     }
     return plan, gates, (wide, wide, rest)
 
@@ -131,17 +131,18 @@
     for name, kind, cols in plan:
         width = cols // 128
         gate = [gates[name]] if name in gates else []
+        late = [("mg", d, line - 1) for d in "ud"] if name in gates else []
         if kind == "A":
             for t in steps:
                 for d in "ud":
                     deps = [(name, d, t - 1)] if t > 1 else [(name, "1")] + gate
                     out[(name, d, t)] = dict(link="z" + d, size=2 * width, deps=deps, phase="z")
-            out[(name, "y", "o", 0)] = dict(link="y", size=2 * width, deps=[(name, "1")], phase="y")
+            out[(name, "y", "o", 0)] = dict(link="y", size=2 * width, deps=[(name, "1")] + late, phase="y")
             for t in steps:
                 for d in "ud":
                     out[(name, "y", d, t)] = dict(link="y", size=2 * width, deps=[(name, d, t)], phase="y")
         else:
-            out[(name, "y", "o", 0)] = dict(link="y", size=2 * width, deps=[(name, "1")], phase="y")
+            out[(name, "y", "o", 0)] = dict(link="y", size=2 * width, deps=[(name, "1")] + late, phase="y")
             for t in steps:
                 for d in "ud":
                     deps = [(name, d, t - 1)] if t > 1 else [(name, "y", "o", 0)] + gate
@@ -157,7 +158,8 @@
         for key, item in transfers.items():
             if key not in arrival and all(dep in seen for dep in item["deps"]):
                 start = max(now, free.get(item["link"], 0.0))
-                free[item["link"]] = start + item["size"] * UNIT_US
+                share = 0.5 if key[1] == "y" and key[2] != "o" else 1.0
+                free[item["link"]] = start + share * item["size"] * UNIT_US
                 arrival[key] = free[item["link"]] + HOP_US
                 program.append(("send", key))
                 if key == ("mo", "1"):
@@ -195,30 +197,32 @@
 
 def compute_list():
     items = [
-        ("tok_fwd", (), (), 0.2, 10.0),
-        ("norm1", (), ("tok_fwd",), 2.0, 1.5),
-        ("mixv", ("mv",), ("norm1",), 0.8, 0.0),
-        ("mixg", ("mg",), ("mixv",), 1.0, 0.0),
-        ("conv_a", (), ("mixg",), 1.2, 0.0),
-        ("conv_b", (), ("conv_a",), 1.2, 0.0),
-        ("stats", (), ("conv_b",), 0.7, 0.0),
-        ("active", (), ("stats",), 1.5, 2.5),
-        ("out_far", ("mo",), ("active",), 0.8, 0.0),
-        ("out_near", (), ("out_far",), 0.8, 0.0),
-        ("out_x", (), ("out_near",), 0.5, 0.8),
-        ("middle", (), ("out_x",), 0.8, 8.0),
+        ("norm1_near", (), (), 1.2, 4.0),
+        ("tok_fwd", (), (), 0.2, 9.5),
+        ("norm1_far", (), ("tok_fwd",), 1.2, 1.2),
+        ("mixv", ("mv",), ("norm1_near", "norm1_far"), 0.7, 0.0),
+        ("mixg", ("mg",), ("mixv",), 0.7, 0.0),
+        ("conv_a", (), ("mixg",), 1.7, 0.0),
+        ("conv_b", (), ("conv_a",), 1.7, 0.0),
+        ("stats", (), ("conv_b",), 0.4, 0.0),
+        ("active_far", (), ("stats",), 0.6, 3.0),
+        ("out_far", ("mo",), ("active_far",), 0.6, 0.0),
+        ("active_near", (), ("out_far",), 0.6, 0.0),
+        ("out_near", (), ("active_near",), 1.0, 0.0),
+        ("out_x", (), ("out_near",), 0.4, 0.8),
+        ("middle", (), ("out_x",), 0.6, 11.5),
+        ("norm2_near", (), ("middle",), 1.2, 1.2),
         ("mid_fwd", (), ("middle",), 0.2, 8.0),
-        ("norm2", (), ("mid_fwd",), 2.0, 1.5),
+        ("norm2_far", (), ("mid_fwd",), 1.2, 1.2),
     ]
-    for g in (0, 1, 2):
-        items.append(("up%d" % g, ("vg%d" % g,), ("norm2",), (2.0, 2.0, 1.0)[g], 0.0))
-    for g in (0, 1, 2):
-        items.append(("down_far%d" % g, ("w%d" % g,), ("up%d" % g,), 0.5, 0.0))
-    items.append(("send_far", (), tuple("down_far%d" % g for g in (0, 1, 2)), 0.1, 0.0))
-    for g in (0, 1, 2):
-        items.append(("down_near%d" % g, (), ("send_far", ), 0.5, 0.0))
-    items.append(("down_x", (), tuple("down_near%d" % g for g in (0, 1, 2)), 0.5, 0.0))
-    items.append(("finish", (), ("down_x",), 1.0, 7.5))
+    for side in ("far", "near"):
+        for g in (0, 1, 2):
+            items.append(("up_%s%d" % (side, g), ("vg%d" % g,), ("norm2_" + side,), (0.8, 0.8, 0.5)[g], 0.0))
+        for g in (0, 1, 2):
+            items.append(("down_%s%d" % (side, g), ("w%d" % g,), ("up_%s%d" % (side, g),), 0.4, 0.0))
+        items.append(("send_" + side, (), tuple("down_%s%d" % (side, g) for g in (0, 1, 2)), 0.1, 0.0))
+    items.append(("down_x", (), ("send_far",), 0.5, 1.0))
+    items.append(("finish", (), ("down_x", "send_near"), 1.0, 7.5))
     return items
 
 
@@ -354,26 +358,25 @@
     down_near = exchange(down_near_peer, down_near_in, down_near_in, tp=peer)
     down_x = exchange(down_x_out, down_x_in, down_x_in, fs=at_x)
 
-    def norm_rows(rows_of, gain):
-        for side in (0, 1):
-            def block(r, carry):
-                at_rows = pl.ds(pl.multiple_of(r * 32, 32), 32)
-                a = rows_of[side, 0, at_rows, :].astype(jnp.float32)
-                b = rows_of[side, 1, at_rows, :].astype(jnp.float32)
-                total = jnp.sum(a * a + b * b, axis=-1, keepdims=True)
-                scale = lax.rsqrt(total / width + EPS)
-                normed[0, side, at_rows, :] = (a * scale * gain[0]).astype(jnp.bfloat16)
-                normed[1, side, at_rows, :] = (b * scale * gain[1]).astype(jnp.bfloat16)
-                return carry
-
-            lax.fori_loop(0, tok_rows // 32, block, 0)
-
-    def project(name, lo, hi):
+    def norm_rows(rows_of, gain, side):
+        def block(r, carry):
+            at_rows = pl.ds(pl.multiple_of(r * 64, 64), 64)
+            a = rows_of[side, 0, at_rows, :].astype(jnp.float32)
+            b = rows_of[side, 1, at_rows, :].astype(jnp.float32)
+            total = jnp.sum(a * a + b * b, axis=-1, keepdims=True)
+            scale = lax.rsqrt(total / width + EPS)
+            normed[0, side, at_rows, :] = (a * scale * gain[0]).astype(jnp.bfloat16)
+            normed[1, side, at_rows, :] = (b * scale * gain[1]).astype(jnp.bfloat16)
+            return carry
+
+        lax.fori_loop(0, tok_rows // 64, block, 0)
+
+    def project(name, lo, hi, side=None):
         total = None
         for h in (0, 1):
             weight = held[name][h * half:(h + 1) * half, :, :, :, lo:hi]
             weight = weight.reshape(-1, hi - lo)
-            left = normed[h].reshape(2 * tok_rows, tok_cols)
+            left = normed[h].reshape(2 * tok_rows, tok_cols) if side is None else normed[h, side]
             term = jnp.dot(left, weight, preferred_element_type=jnp.float32)
             total = term if total is None else total + term
         return total
@@ -391,11 +394,14 @@
         tok_x[1]()
         tok_fwd[0]()
 
-    def norm1():
+    def norm1_near():
         pad[...] = jnp.zeros_like(pad)
         tok_core[1]()
+        norm_rows(tokall, gain1, x)
+
+    def norm1_far():
         tok_fwd[1]()
-        norm_rows(tokall, gain1)
+        norm_rows(tokall, gain1, far)
 
     seqs = 2 * tok_rows // SEQ_LEN
     lead = -(-(taps // 2) // 8) * 8
@@ -432,18 +438,18 @@
         for send, _ in stat_all:
             send()
 
-    def make_active():
-        for _, wait in stat_all:
-            wait()
-        for r in range(0, 2 * tok_rows, 128):
-            both = stat[:, r:r + 128] + stats_in[0, :, r:r + 128] + (
-                stats_in[1, :, r:r + 128] + stats_in[2, :, r:r + 128]
-            )
+    def make_active(side, first):
+        if first:
+            for _, wait in stat_all:
+                wait()
+        for r in range(0, tok_rows, 128):
+            at_rows = pl.ds(pl.multiple_of(side * tok_rows + r, 128), 128)
+            both = stat[:, at_rows] + stats_in[0, :, at_rows] + (stats_in[1, :, at_rows] + stats_in[2, :, at_rows])
             both = jnp.concatenate([both] * 16, axis=0).T
             mean = both[:, 0:1] / (4 * mix_cols)
             var = jnp.maximum(both[:, 1:2] / (4 * mix_cols) - mean * mean, 0.0)
-            v = (mixed[r:r + 128, :] - mean) * lax.rsqrt(var + EPS) * cgain[x] + cbias[x]
-            active[r:r + 128, :] = (v * jax.nn.sigmoid(v)).astype(jnp.bfloat16)
+            v = (mixed[at_rows, :] - mean) * lax.rsqrt(var + EPS) * cgain[x] + cbias[x]
+            active[at_rows, :] = (v * jax.nn.sigmoid(v)).astype(jnp.bfloat16)
 
     def rows_at(side):
         return pl.ds(pl.multiple_of(side * tok_rows, tok_rows), tok_rows)
@@ -455,11 +461,11 @@
         far_mine[...] = project_back(left, "mo", core)
 
     def make_out_near():
+        out_far[1]()
+        x_out[...] = far_mine[...] + far_in[...]
+        out_x[0]()
         left = active[rows_at(x), :]
         near_peer[...] = project_back(left, "mo", peer)
-        out_far[1]()
-        x_out[...] = (far_mine[...] + far_in[...]).astype(jnp.bfloat16)
-        out_x[0]()
         out_near[0]()
         near_mine[...] = project_back(left, "mo", core)
 
@@ -469,7 +475,7 @@
 
     def make_middle():
         out_x[1]()
-        total = tokens[...].astype(jnp.float32) + (near_mine[...] + x_in[...].astype(jnp.float32))
+        total = tokens[...].astype(jnp.float32) + (near_mine[...] + x_in[...])
         midall[x, core] = total.astype(jnp.bfloat16)
         mid_x[0]()
         mid_core[0]()
@@ -478,10 +484,13 @@
         mid_x[1]()
         mid_fwd[0]()
 
-    def norm2():
+    def norm2_near():
         mid_core[1]()
+        norm_rows(midall, gain2, x)
+
+    def norm2_far():
         mid_fwd[1]()
-        norm_rows(midall, gain2)
+        norm_rows(midall, gain2, far)
 
     def short_conv(values, kernel_rows, lanes):
         pos = lax.rem(lax.broadcasted_iota(jnp.int32, values.shape, 0), SEQ_LEN)
@@ -490,28 +499,28 @@
             shift = k - ffn_taps // 2
             term = values
             if shift:
-                term = pltpu.roll(values, (-shift) % (2 * tok_rows), 0)
+                term = pltpu.roll(values, (-shift) % tok_rows, 0)
                 inside = pos < SEQ_LEN - shift if shift > 0 else pos >= -shift
                 term = jnp.where(inside, term, 0.0)
             term = term * kernel_rows[k:k + 1, lanes]
             total = term if total is None else total + term
         return total
 
-    def up(g):
+    def up(g, side):
         count = groups[g]
         start = sum(groups[:g])
         for c in range(0, count, 256):
             n = min(256, count - c)
             lanes = pl.ds(pl.multiple_of(x * ffn_cols + start + c, 128), n)
             name = "vg%d" % g
-            value = short_conv(project(name, c, c + n), vkern, lanes)
-            gate = short_conv(project(name, count + c, count + c + n), gkern, lanes)
-            hidden[g][:, c:c + n] = (gate * jax.nn.sigmoid(gate) * value).astype(jnp.bfloat16)
+            value = short_conv(project(name, c, c + n, side), vkern, lanes)
+            gate = short_conv(project(name, count + c, count + c + n, side), gkern, lanes)
+            hidden[g][side, :, c:c + n] = (gate * jax.nn.sigmoid(gate) * value).astype(jnp.bfloat16)
 
     fresh = set()
 
     def down(g, where, name, peer_buf, mine_buf):
-        left = hidden[g][rows_at(where), :]
+        left = hidden[g][where]
         for side, buf in ((peer, peer_buf), (core, mine_buf)):
             term = project_back(left, "w%d" % g, side)
             if name in fresh:
@@ -521,7 +530,6 @@
         fresh.add(name)
 
     def make_down_x():
-        down_near[0]()
         down_far[1]()
         down_x_out[...] = (down_far_mine[...] + down_far_in[...]).astype(jnp.bfloat16)
         down_x[0]()
@@ -534,14 +542,16 @@
         out[...] = (down_near_mine[...] + down_x_in[...].astype(jnp.float32)).astype(jnp.bfloat16)
 
     run = {
-        "tok_start": start_tokens, "tok_fwd": forward_tokens, "norm1": norm1, "mixv": mixv, "mixg": mixg,
-        "conv_a": lambda: conv(0, seqs // 2), "conv_b": lambda: conv(seqs // 2, seqs),
-        "stats": stats, "active": make_active, "out_far": make_out_far, "out_near": make_out_near,
-        "out_x": make_out_x, "middle": make_middle, "mid_fwd": forward_middle, "norm2": norm2,
-        "send_far": down_far[0], "down_x": make_down_x, "finish": finish,
+        "tok_start": start_tokens, "tok_fwd": forward_tokens, "norm1_near": norm1_near, "norm1_far": norm1_far,
+        "mixv": mixv, "mixg": mixg, "conv_a": lambda: conv(0, seqs // 2), "conv_b": lambda: conv(seqs // 2, seqs),
+        "stats": stats, "active_far": lambda: make_active(far, True), "active_near": lambda: make_active(x, False),
+        "out_far": make_out_far, "out_near": make_out_near, "out_x": make_out_x, "middle": make_middle,
+        "mid_fwd": forward_middle, "norm2_near": norm2_near, "norm2_far": norm2_far,
+        "send_far": down_far[0], "send_near": down_near[0], "down_x": make_down_x, "finish": finish,
     }
     for g in (0, 1, 2):
-        run["up%d" % g] = functools.partial(up, g)
+        run["up_far%d" % g] = functools.partial(up, g, far)
+        run["up_near%d" % g] = functools.partial(up, g, x)
         run["down_far%d" % g] = functools.partial(down, g, far, "far", down_far_peer, down_far_mine)
         run["down_near%d" % g] = functools.partial(down, g, x, "near", down_near_peer, down_near_mine)
 
@@ -587,12 +597,12 @@
     lead = -(-(mix_kernel.shape[0] // 2) // 8) * 8
     both = 2 * tok_rows
     full = (tok_rows, tok_cols)
-    sums = [vm(full, f32)] * 6 + [vm(full, bf16)] * 2
+    sums = [vm(full, f32)] * 6
     scratch = [vm((line, 2, 2, rows, item[2]), bf16) for item in plan] + [
         vm((2, 2) + full, bf16), vm((2, 2) + full, bf16), vm((2, 2) + full, bf16),
         vm((both, mix_cols), f32), vm((both // SEQ_LEN, SEQ_LEN + 2 * lead, mix_cols), f32),
         vm((both, mix_cols), f32), vm((8, both), f32), vm((3, 8, both), f32), vm((both, mix_cols), bf16),
-    ] + sums + [vm((both, g), bf16) for g in groups] + sums + [
+    ] + sums + [vm(full, f32)] * 2 + [vm((2, tok_rows, g), bf16) for g in groups] + sums + [vm(full, bf16)] * 2 + [
         pltpu.SemaphoreType.DMA((len(transfers),)), pltpu.SemaphoreType.DMA((len(transfers),)),
         pltpu.SemaphoreType.DMA((len(plan) + 1,)), pltpu.SemaphoreType.DMA((15,)), pltpu.SemaphoreType.DMA((15,)),
     ]

time: 103 us -> 87.1 us (0.85)
  Pallas kernels: 96.4 us -> 79.9 us
    pallas_call x1, Pallas kernels: 96.4 us -> 79.9 us  [fused_body(): pl.pallas_call(functools.partial(layer_kernel, sizes, plan, groups, trans...]
where the time goes in v3:
time: 87.1 us; the launch traced here: 86.7 us
  Pallas kernels  79.9 us (92%)
  local copies, waits for them, and re-layouts  3.64 us (4%)
  other arithmetic  2.9 us (3%)
    pallas_call x1, Pallas kernels, fused_body(): pl.pallas_call(functools.partial(layer_kernel, sizes, plan, groups, trans...  79.9 us
    unnamed x28, local copies, waits for them, and re-layouts  3.62 us
    another operation x6, other arithmetic  2.9 us

profile of v3, /device:TPU:0, one launch (start us, length us, event | category | flops | bytes accessed | tf_op | source)
XLA Modules:
  0.0 86.7 jit_solution(9114707684850505847)
XLA Ops:
  0.0 0.0 copy-start.1
  0.0 1.0 %convert.32 = bf16[64,512]{1,0:T(8,128)(2,1)S(1)} convert(f32[64,512]{1,0:T(8,128)} %param.16) | non-fusion elementwise | flops 32768 | bytes 196608 | tf_op jit(solution)/shard_map/convert.19
  1.0 0.9 %convert.33 = bf16[64,512]{1,0:T(8,128)(2,1)S(1)} convert(f32[64,512]{1,0:T(8,128)} %param.17) | non-fusion elementwise | flops 32768 | bytes 196608 | tf_op jit(solution)/shard_map/convert.18
  1.9 0.0 copy-start.2
  1.9 1.0 %convert_bitcast_fusion.1 = bf16[64,512]{1,0:T(8,128)(2,1)S(1)} fusion(f32[512,64]{0,1:T(8,128)} %param.21), kind=kLoop, calls=%fused_computation.3 | loop fusion | flops 32768 | bytes 196608 | tf_op jit(solution)/shard_map/convert.17
  2.9 0.0 copy-done.1
  2.9 0.0 copy-done.2
  2.9 0.0 copy-start.3
  3.0 0.9 %copy-done.3 = f32[1280,64]{0,1:T(8,128)S(1)} copy-done((f32[1280,64]{0,1:T(8,128)S(1)}, f32[1280,64]{0,1:T(8,128)}, u32[]{:S(2)}) %copy-start.3) | copy-done | bytes 327704
  4.2 0.0 copy-start
  4.2 0.8 copy-done
  5.1 79.9 %shard_map.136 = bf16[256,512]{1,0:T(8,128)(2,1)} custom-call(bf16[256,512]{1,0:T(8,128)(2,1)} %refs_0_.1, f32[2,1,512]{2,1,0:T(1,128)} %bitcast.8, f32[31,512]{1,0:T(8,128)} %refs_2_.1, f32[2,1,256]{2,1,0:T(1,128)} %bitcast.10, f32[2,1,256]{2,1,0:T(1,128)} %bitcast.11, f32[2,1,512]{2,1,0:T(1,128)} %bitcast.9, f32[3,1280]{1,0:T(4,128)} %refs_6_.1, ...), custom_call_target="tpu_custom_call" | custom-call | tf_op jit(solution)/shard_map/pallas_call | solution.py:609
  85.0 1.7 %copy.35 = bf16[256,512]{1,0:T(8,128)(2,1)} copy(bf16[256,512]{1,0:T(8,128)(2,1)} %shard_map.136) | data formatting | bytes 524288
  (23 shorter events, 0.2 us)
Async XLA Ops:
  0.0 2.9 %copy-start.1 = (f32[64,1280]{1,0:T(8,128)S(1)}, f32[64,1280]{1,0:T(8,128)}, u32[]{:S(2)}) copy-start(f32[64,1280]{1,0:T(8,128)} %param.23) | copy-start | bytes 983044
  1.9 1.0 %copy-start.2 = (f32[64,1280]{1,0:T(8,128)S(1)}, f32[64,1280]{1,0:T(8,128)}, u32[]{:S(2)}) copy-start(f32[64,1280]{1,0:T(8,128)} %param.24) | copy-start | bytes 983044
  2.9 1.0 %copy-start.3 = (f32[1280,64]{0,1:T(8,128)S(1)}, f32[1280,64]{0,1:T(8,128)}, u32[]{:S(2)}) copy-start(f32[1280,64]{0,1:T(8,128)} %param.27) | copy-start | bytes 983044
  4.2 0.9 copy-start

commit v4 on v3

--- a/solution.py
+++ b/solution.py
@@ -117,8 +117,8 @@
         ("w0", "A", wide), ("w1", "A", wide), ("w2", "B", rest),
     ]
     gates = {
-        "vg0": ("mo", "u", 1), "vg1": ("vg0", "u", 1), "vg2": ("vg1", "u", 1), "w0": ("vg2", "u", 1),
-        "w1": ("w0", "u", 1), "w2": ("w1", "u", 1),
+        "vg0": ("mo", "u", 2), "vg1": ("vg0", "u", 1), "vg2": ("mg", "u", 2), "w0": ("mo", "u", 1),
+        "w1": ("vg0", "u", 1), "w2": ("vg0", "u", 2),
     }
     return plan, gates, (wide, wide, rest)
 
@@ -210,9 +210,10 @@
         ("active_near", (), ("out_far",), 0.6, 0.0),
         ("out_near", (), ("active_near",), 1.0, 0.0),
         ("out_x", (), ("out_near",), 0.4, 0.8),
-        ("middle", (), ("out_x",), 0.6, 11.5),
+        ("middle_a", (), ("out_x",), 0.4, 5.6),
+        ("middle", (), ("middle_a",), 0.4, 5.4),
         ("norm2_near", (), ("middle",), 1.2, 1.2),
-        ("mid_fwd", (), ("middle",), 0.2, 8.0),
+        ("mid_fwd", (), ("middle",), 0.2, 5.5),
         ("norm2_far", (), ("mid_fwd",), 1.2, 1.2),
     ]
     for side in ("far", "near"):
@@ -344,7 +345,10 @@
     tok_x = exchange(tokens, tokall.at[x, core], tokall.at[far, core], fs=at_x)
     tok_fwd = exchange(tokall.at[far, core], tokall.at[far, core], tokall.at[far, peer], tp=peer)
     mid_core = exchange(midall.at[x, core], midall.at[x, core], midall.at[x, peer], tp=peer)
-    mid_x = exchange(midall.at[x, core], midall.at[x, core], midall.at[far, core], fs=at_x)
+    mid_x = [
+        exchange(midall.at[x, core, r], midall.at[x, core, r], midall.at[far, core, r], fs=at_x)
+        for r in (pl.ds(0, tok_rows // 2), pl.ds(tok_rows // 2, tok_rows // 2))
+    ]
     mid_fwd = exchange(midall.at[far, core], midall.at[far, core], midall.at[far, peer], tp=peer)
     stat_all = [
         exchange(stat, stats_in.at[0], stats_in.at[0], tp=peer),
@@ -353,7 +357,9 @@
     ]
     out_far = exchange(far_peer, far_in, far_in, tp=peer)
     out_near = exchange(near_peer, near_in, near_in, tp=peer)
-    out_x = exchange(x_out, x_in, x_in, fs=at_x)
+    cut = tok_rows // 2
+    top, low = pl.ds(0, cut), pl.ds(cut, cut)
+    out_x = [exchange(x_out.at[r], x_in.at[r], x_in.at[r], fs=at_x) for r in (top, low)]
     down_far = exchange(down_far_peer, down_far_in, down_far_in, tp=peer)
     down_near = exchange(down_near_peer, down_near_in, down_near_in, tp=peer)
     down_x = exchange(down_x_out, down_x_in, down_x_in, fs=at_x)
@@ -463,7 +469,8 @@
     def make_out_near():
         out_far[1]()
         x_out[...] = far_mine[...] + far_in[...]
-        out_x[0]()
+        out_x[0][0]()
+        out_x[1][0]()
         left = active[rows_at(x), :]
         near_peer[...] = project_back(left, "mo", peer)
         out_near[0]()
@@ -473,15 +480,17 @@
         out_near[1]()
         near_mine[...] += near_in[...]
 
-    def make_middle():
-        out_x[1]()
-        total = tokens[...].astype(jnp.float32) + (near_mine[...] + x_in[...])
-        midall[x, core] = total.astype(jnp.bfloat16)
-        mid_x[0]()
-        mid_core[0]()
+    def make_middle(part, rows):
+        out_x[part][1]()
+        total = tokens[rows, :].astype(jnp.float32) + (near_mine[rows, :] + x_in[rows, :])
+        midall[x, core, rows, :] = total.astype(jnp.bfloat16)
+        mid_x[part][0]()
+        if part:
+            mid_core[0]()
 
     def forward_middle():
-        mid_x[1]()
+        mid_x[0][1]()
+        mid_x[1][1]()
         mid_fwd[0]()
 
     def norm2_near():
@@ -545,7 +554,7 @@
         "tok_start": start_tokens, "tok_fwd": forward_tokens, "norm1_near": norm1_near, "norm1_far": norm1_far,
         "mixv": mixv, "mixg": mixg, "conv_a": lambda: conv(0, seqs // 2), "conv_b": lambda: conv(seqs // 2, seqs),
         "stats": stats, "active_far": lambda: make_active(far, True), "active_near": lambda: make_active(x, False),
-        "out_far": make_out_far, "out_near": make_out_near, "out_x": make_out_x, "middle": make_middle,
+        "out_far": make_out_far, "out_near": make_out_near, "out_x": make_out_x, "middle_a": lambda: make_middle(0, top), "middle": lambda: make_middle(1, low),
         "mid_fwd": forward_middle, "norm2_near": norm2_near, "norm2_far": norm2_far,
         "send_far": down_far[0], "send_near": down_near[0], "down_x": make_down_x, "finish": finish,
     }
@@ -604,7 +613,7 @@
         vm((both, mix_cols), f32), vm((8, both), f32), vm((3, 8, both), f32), vm((both, mix_cols), bf16),
     ] + sums + [vm(full, f32)] * 2 + [vm((2, tok_rows, g), bf16) for g in groups] + sums + [vm(full, bf16)] * 2 + [
         pltpu.SemaphoreType.DMA((len(transfers),)), pltpu.SemaphoreType.DMA((len(transfers),)),
-        pltpu.SemaphoreType.DMA((len(plan) + 1,)), pltpu.SemaphoreType.DMA((15,)), pltpu.SemaphoreType.DMA((15,)),
+        pltpu.SemaphoreType.DMA((len(plan) + 1,)), pltpu.SemaphoreType.DMA((17,)), pltpu.SemaphoreType.DMA((17,)),
     ]
     return pl.pallas_call(
         functools.partial(layer_kernel, sizes, plan, groups, transfers, program),

time: 87.1 us -> 85 us (0.976)
  Pallas kernels: 79.9 us -> 77.8 us
    pallas_call x1, Pallas kernels: 79.9 us -> 77.8 us  [fused_body(): pl.pallas_call(functools.partial(layer_kernel, sizes, plan, groups, trans...]
where the time goes in v4:
time: 85 us; the launch traced here: 84.5 us
  Pallas kernels  77.8 us (92%)
  local copies, waits for them, and re-layouts  3.64 us (4%)
  other arithmetic  2.9 us (3%)
    pallas_call x1, Pallas kernels, fused_body(): pl.pallas_call(functools.partial(layer_kernel, sizes, plan, groups, trans...  77.8 us
    unnamed x28, local copies, waits for them, and re-layouts  3.62 us
    another operation x6, other arithmetic  2.9 us

profile of v4, /device:TPU:0, one launch (start us, length us, event | category | flops | bytes accessed | tf_op | source)
XLA Modules:
  0.0 84.5 jit_solution(10277827863494974405)
XLA Ops:
  0.0 0.0 copy-start.1
  0.0 1.0 %convert.32 = bf16[64,512]{1,0:T(8,128)(2,1)S(1)} convert(f32[64,512]{1,0:T(8,128)} %param.16) | non-fusion elementwise | flops 32768 | bytes 196608 | tf_op jit(solution)/shard_map/convert.19
  1.0 0.9 %convert.33 = bf16[64,512]{1,0:T(8,128)(2,1)S(1)} convert(f32[64,512]{1,0:T(8,128)} %param.17) | non-fusion elementwise | flops 32768 | bytes 196608 | tf_op jit(solution)/shard_map/convert.18
  1.9 0.0 copy-start.2
  1.9 1.0 %convert_bitcast_fusion.1 = bf16[64,512]{1,0:T(8,128)(2,1)S(1)} fusion(f32[512,64]{0,1:T(8,128)} %param.21), kind=kLoop, calls=%fused_computation.3 | loop fusion | flops 32768 | bytes 196608 | tf_op jit(solution)/shard_map/convert.17
  2.9 0.0 copy-done.1
  2.9 0.0 copy-done.2
  2.9 0.0 copy-start.3
  3.0 0.9 %copy-done.3 = f32[1280,64]{0,1:T(8,128)S(1)} copy-done((f32[1280,64]{0,1:T(8,128)S(1)}, f32[1280,64]{0,1:T(8,128)}, u32[]{:S(2)}) %copy-start.3) | copy-done | bytes 327704
  4.2 0.0 copy-start
  4.2 0.8 copy-done
  5.1 77.8 %shard_map.136 = bf16[256,512]{1,0:T(8,128)(2,1)} custom-call(bf16[256,512]{1,0:T(8,128)(2,1)} %refs_0_.1, f32[2,1,512]{2,1,0:T(1,128)} %bitcast.8, f32[31,512]{1,0:T(8,128)} %refs_2_.1, f32[2,1,256]{2,1,0:T(1,128)} %bitcast.10, f32[2,1,256]{2,1,0:T(1,128)} %bitcast.11, f32[2,1,512]{2,1,0:T(1,128)} %bitcast.9, f32[3,1280]{1,0:T(4,128)} %refs_6_.1, ...), custom_call_target="tpu_custom_call" | custom-call | tf_op jit(solution)/shard_map/pallas_call | solution.py:618
  82.8 1.7 %copy.35 = bf16[256,512]{1,0:T(8,128)(2,1)} copy(bf16[256,512]{1,0:T(8,128)(2,1)} %shard_map.136) | data formatting | bytes 524288
  (23 shorter events, 0.2 us)
Async XLA Ops:
  0.0 2.9 %copy-start.1 = (f32[64,1280]{1,0:T(8,128)S(1)}, f32[64,1280]{1,0:T(8,128)}, u32[]{:S(2)}) copy-start(f32[64,1280]{1,0:T(8,128)} %param.23) | copy-start | bytes 983044
  1.9 1.0 %copy-start.2 = (f32[64,1280]{1,0:T(8,128)S(1)}, f32[64,1280]{1,0:T(8,128)}, u32[]{:S(2)}) copy-start(f32[64,1280]{1,0:T(8,128)} %param.24) | copy-start | bytes 983044
  2.9 1.0 %copy-start.3 = (f32[1280,64]{0,1:T(8,128)S(1)}, f32[1280,64]{0,1:T(8,128)}, u32[]{:S(2)}) copy-start(f32[1280,64]{0,1:T(8,128)} %param.27) | copy-start | bytes 983044
  4.2 0.9 %copy-start = (bf16[64,5376]{1,0:T(8,128)(2,1)}, bf16[64,5376]{1,0:T(8,128)(2,1)S(1)}, u32[]{:S(2)}) copy-start(bf16[64,5376]{1,0:T(8,128)(2,1)S(1)} %slice_dynamic-update-slice_fusion.refs_8_) | copy-start | bytes 2064388
